TPU v7x, 512 devices: a whole 4x4x16 slice. The times are simulated.
512 devices in a mesh: fs: 32 (over z, core), tp: 16 (over y, x).
Axes of the slice: x: 4, y: 4, z: 16, core: 2. Of those that a mesh axis runs over, the one named last changes fastest.
Arguments:
- tokens: bfloat16 [4096, 2048], P('fs'), may hold values from -6 to 6
- experts: int32 [4096, 4], P('fs'), may hold values from 0 to 31, all different within a row; in each aligned block of 128 rows (0 to 127, 128 to 255, ...) at most 24 rows name the same one
- routing: float32 [4096, 4], P('fs'), may hold values from 0.05 to 0.6
- norm_gain: float32 [2048], replicated, may hold values from 0.1 to 1.9
- gate_master: float32 [32, 2048, 2048], P(None, 'fs', 'tp'), may hold values from -0.625 to 0.625
- linear_master: float32 [32, 2048, 2048], P(None, 'fs', 'tp'), may hold values from -0.625 to 0.625
- down_weight: bfloat16 [32, 2048, 2048], P('fs', None, 'tp'), may hold values from -0.013671875 to 0.013671875
Outputs:
- gate_out: bfloat16 [32, 2048, 2048], P('fs', None, 'tp')
- linear_out: bfloat16 [32, 2048, 2048], P('fs', None, 'tp')
- expert_mix: bfloat16 [4096, 2048], P('fs', 'tp')
Inputs may be any that keep to these rules, and one draw needn't show every extreme that they name: Each row names 4 different experts; within the rows of one index of fs (aligned blocks of 128 rows) no expert is named by more than 24 rows, and in some blocks some expert is named by exactly 24; every expert is named somewhere.
All inputs are finite; a program needn't handle non-finite values.
Results may differ from a plain program's by a relative error of at most 0.023.
Values may be sent and summed in bfloat16 or wider, within the bound.
A program may use at most 64 MiB of HBM per device.

v0:
```python
import jax
import jax.numpy as jnp
from jax import lax
from jax.sharding import Mesh
from jax.sharding import PartitionSpec as P

FS = ("fs_0", "fs_1")


clamp_limit = 7.0
gate_slope = 1.702


def in_one_piece(arrays, axis, split_dim, concat_dim, along):
    both = jnp.concatenate(arrays, axis=along)
    filled, at, finished = (
        lax.all_to_all(both, axis, split_axis=split_dim, concat_axis=concat_dim, tiled=True),
        0,
        [],
    )
    for a in arrays:
        finished.append(lax.slice_in_dim(filled, at, at + a.shape[along], axis=along))
        at += a.shape[along]
    return tuple(finished)


def in_blocks(shard, dim, peers):
    dims = shard.shape
    blocks = shard.reshape(*dims[:dim], peers, dims[dim] // peers, *dims[dim + 1 :])
    return jnp.moveaxis(blocks, dim, 0)


def summed_on_arrival(shard, axis, dim):
    peers = lax.axis_size(axis)
    blocks = lax.all_to_all(in_blocks(shard, dim, peers), axis, 0, 0, tiled=True)
    return jnp.sum(blocks.astype(jnp.float32), axis=0)


def laid_out(blocks, dim):
    dims = list(blocks.shape[1:])
    dims[dim] *= blocks.shape[0]
    return jnp.moveaxis(blocks, 0, dim).reshape(dims)


def exchange_in_order(blocks, axes, turns):
    inside = blocks.shape[1:]
    filled = blocks.reshape(*(lax.axis_size(a) for a in axes), *inside)
    for k in turns:
        filled = lax.all_to_all(filled, axes[k], k, k, tiled=True)
    return filled.reshape(-1, *inside)


def exchange_by_chip(shard, groups, turns, split_dim, concat_dim):
    peers = lax.axis_size(groups[0]) * lax.axis_size(groups[1])
    blocks = in_blocks(shard, split_dim, peers)
    return laid_out(exchange_in_order(blocks, groups, turns), concat_dim)


def on_device(tokens, experts, routing, norm_gain, gate_master, linear_master, down_weight):
    tok_count, top_count = experts.shape
    expert_count = gate_master.shape[0]
    width = tokens.shape[1]
    capacity = 3 * tok_count * top_count // (2 * expert_count)
    stripe = gate_master.shape[1]
    local_gain = lax.dynamic_slice_in_dim(norm_gain, lax.axis_index(FS) * stripe, stripe)[
        None, :, None
    ]
    gate_out, linear_out = in_one_piece(
        (
            (gate_master * local_gain).astype(jnp.bfloat16),
            (linear_master * local_gain).astype(jnp.bfloat16),
        ),
        FS,
        0,
        1,
        2,
    )
    flat_ids = experts.reshape(-1)
    one_hot = (flat_ids[:, None] == jnp.arange(expert_count, dtype=jnp.int32)[None, :]).astype(
        jnp.int32
    )
    slot_rank = jnp.sum((jnp.cumsum(one_hot, axis=0) - one_hot) * one_hot, axis=1)
    slot_index = flat_ids * capacity + slot_rank
    owner = jnp.arange(tok_count * top_count, dtype=jnp.int32) // top_count
    slot_token = (
        jnp.full((expert_count * capacity,), tok_count, jnp.int32).at[slot_index].set(owner)
    )
    padded = jnp.concatenate([tokens, jnp.zeros((1, width), tokens.dtype)], axis=0)
    sender = padded[slot_token].reshape(expert_count, capacity, width)
    gate_local = gate_out[0]
    linear_local = linear_out[0]
    down_local = down_weight[0]
    item_rows = lax.all_to_all(sender, FS, split_axis=0, concat_axis=0, tiled=True)
    flat_rows = item_rows.reshape(-1, width)
    pre_gate = jnp.dot(flat_rows, gate_local, preferred_element_type=jnp.float32)
    pre_linear = jnp.dot(flat_rows, linear_local, preferred_element_type=jnp.float32)
    clamped = jnp.minimum(pre_gate, clamp_limit)
    active = (
        clamped
        * jax.nn.sigmoid(gate_slope * clamped)
        * (jnp.clip(pre_linear, -clamp_limit, clamp_limit) + 1.0)
    ).astype(jnp.bfloat16)
    partial_value = lax.dot_general(
        active, down_local, (((1,), (1,)), ((), ())), preferred_element_type=jnp.float32
    ).reshape(item_rows.shape)
    results = partial_value.astype(jnp.bfloat16)
    summed = summed_on_arrival(results, "tp", 2)
    returned = exchange_by_chip(summed.astype(jnp.bfloat16), ("fs_0", "fs_1"), (1, 0), 0, 0).astype(
        summed.dtype
    )
    picked = returned.reshape(expert_count * capacity, -1)[slot_index].reshape(
        tok_count, top_count, -1
    )
    expert_mix = jnp.sum(routing[:, :, None] * picked, axis=1).astype(jnp.bfloat16)
    return (gate_out, linear_out, expert_mix)


def solution(mesh):
    torus = Mesh(mesh.devices.reshape(16, 2, mesh.shape["tp"]), ("fs_0", "fs_1", "tp"))
    placed = (
        P(FS, None),
        P(FS, None),
        P(FS, None),
        P(),
        P(None, FS, "tp"),
        P(None, FS, "tp"),
        P(FS, None, "tp"),
    )
    return jax.shard_map(
        on_device,
        mesh=torus,
        in_specs=placed,
        out_specs=(P(FS, None, "tp"), P(FS, None, "tp"), P(FS, "tp")),
        check_vma=False,
    )
```

profile of v0, /device:TPU:1, one launch (start us, length us, event | category | flops | bytes accessed | tf_op | source)
XLA Modules:
  0.0 305.4 jit_solution(6896766847087527402)
XLA Ops:
  0.7 0.8 dynamic_slice.3
  1.5 1.9 multiply_convert_fusion.1
  3.4 1.1 pad_maximum_fusion
  4.5 16.7 %all-to-all-start = ((bf16[32,64,256]{2,1,0:T(8,128)(2,1)}), bf16[32,64,256]{2,1,0:T(8,128)(2,1)S(1)}, u32[]{:S(2)}, u32[]{:S(2)}) async-start(bf16[32,64,256]{2,1,0:T(8,128)(2,1)} %pad_maximum_fusion), calls=%async_computation | async-start | bytes 2097152 | tf_op jit(solution)/shard_map/all_to_all | solution.py:17
  21.3 0.1 copy.25
  21.9 1.2 reduce-window.6
  23.0 0.2 slice_reduce_fusion
  23.5 2.4 scatter_custom_fusion
  26.0 4.3 %gather_fusion = bf16[768,2048]{1,0:T(8,128)(2,1)} fusion(bf16[129,2048]{1,0:T(8,128)(2,1)S(1)} %concatenate.7, s32[1024]{0:T(1024)S(1)} %pad_clamp_fusion.1), kind=kCustom, calls=%fused_computation | custom fusion | bytes 6294528 | tf_op jit(solution)/shard_map/gather | solution.py:89
  30.2 46.7 %all-to-all-done = bf16[32,64,256]{2,1,0:T(8,128)(2,1)S(1)} async-done(((bf16[32,64,256]{2,1,0:T(8,128)(2,1)}), bf16[32,64,256]{2,1,0:T(8,128)(2,1)S(1)}, u32[]{:S(2)}, u32[]{:S(2)}) %all-to-all-start) | async-done | bytes 1048608 | tf_op jit(solution)/shard_map/all_to_all | solution.py:17
  77.0 4.9 %all-to-all-start.1 = ((bf16[32,24,2048]{2,1,0:T(8,128)(2,1)}), bf16[32,24,2048]{2,1,0:T(8,128)(2,1)}, u32[]{:S(2)}, u32[]{:S(2)}) async-start(bf16[32,24,2048]{2,1,0:T(8,128)(2,1)} %bitcast.52), calls=%async_computation.1 | async-start | bytes 6291456 | tf_op jit(solution)/shard_map/all_to_all | solution.py:93
  82.0 141.4 %all-to-all-done.1 = bf16[32,24,2048]{2,1,0:T(8,128)(2,1)} async-done(((bf16[32,24,2048]{2,1,0:T(8,128)(2,1)}), bf16[32,24,2048]{2,1,0:T(8,128)(2,1)}, u32[]{:S(2)}, u32[]{:S(2)}) %all-to-all-start.1) | async-done | bytes 3145760 | tf_op jit(solution)/shard_map/all_to_all | solution.py:93
  223.4 2.9 convolution_minimum_fusion
  226.2 2.9 fusion.3
  229.1 1.0 fusion
  230.2 0.8 copy.35
  231.0 41.1 %all_to_all.32 = bf16[16,32,24,128]{3,2,1,0:T(8,128)(2,1)} all-to-all(bf16[16,32,24,128]{3,2,1,0:T(8,128)(2,1)S(1)} %bitcast.51), channel_id=1, replica_groups=mesh['fs_0'=16,'fs_1'=2,'tp'=16] {'tp'}, dimensions={0} | all-to-all | bytes 6291456 | tf_op jit(solution)/shard_map/all_to_all | solution.py:35
  272.1 2.4 reduce_sum.34
  274.5 10.0 %all_to_all.33 = bf16[16,2,1,24,128]{4,3,0,2,1:T(8,128)(2,1)S(1)} all-to-all(bf16[16,2,1,24,128]{4,3,0,2,1:T(8,128)(2,1)S(1)} %copy.29), channel_id=1, replica_groups=mesh['fs_0'=16,'fs_1'=2,'tp'=16] {'fs_1'}, dimensions={1} | all-to-all | bytes 393216 | tf_op jit(solution)/shard_map/all_to_all | solution.py:49
  284.5 0.7 copy.30
  285.1 6.0 %all-to-all-start.4 = ((bf16[16,2,1,24,128]{4,3,1,2,0:T(8,128)(2,1)}), bf16[16,2,1,24,128]{4,3,1,2,0:T(8,128)(2,1)S(1)}, u32[]{:S(2)}, u32[]{:S(2)}) async-start(bf16[16,2,1,24,128]{4,3,1,2,0:T(8,128)(2,1)} %copy.30), calls=%async_computation.4 | async-start | bytes 393216 | tf_op jit(solution)/shard_map/all_to_all | solution.py:49
  291.2 12.2 %all-to-all-done.4 = bf16[16,2,1,24,128]{4,3,1,2,0:T(8,128)(2,1)S(1)} async-done(((bf16[16,2,1,24,128]{4,3,1,2,0:T(8,128)(2,1)}), bf16[16,2,1,24,128]{4,3,1,2,0:T(8,128)(2,1)S(1)}, u32[]{:S(2)}, u32[]{:S(2)}) %all-to-all-start.4) | async-done | bytes 196640 | tf_op jit(solution)/shard_map/all_to_all | solution.py:49
  303.5 1.0 gather_fusion.1
  304.6 0.9 multiply_reduce_fusion
  (31 shorter events, 0.9 us)
Async XLA Ops:
  0.6 228.5 %copy-start = (bf16[1,2048,128]{2,1,0:T(8,128)(2,1)S(1)}, bf16[1,2048,128]{2,1,0:T(8,128)(2,1)}, u32[]{:S(2)}) copy-start(bf16[1,2048,128]{2,1,0:T(8,128)(2,1)} %param.13) | copy-start | bytes 1572868
  1.5 19.8 %copy-start.4 = (s32[128,4]{0,1:T(4,128)S(1)}, s32[128,4]{0,1:T(4,128)}, u32[]{:S(2)}) copy-start(s32[128,4]{0,1:T(4,128)} %param.8) | copy-start | bytes 6148
  3.4 19.9 %copy-start.2 = (bf16[128,2048]{1,0:T(8,128)(2,1)S(1)}, bf16[128,2048]{1,0:T(8,128)(2,1)}, u32[]{:S(2)}) copy-start(bf16[128,2048]{1,0:T(8,128)(2,1)} %param.7) | copy-start | bytes 1572868
  4.5 72.5 %all-to-all-start = ((bf16[32,64,256]{2,1,0:T(8,128)(2,1)}), bf16[32,64,256]{2,1,0:T(8,128)(2,1)S(1)}, u32[]{:S(2)}, u32[]{:S(2)}) async-start(bf16[32,64,256]{2,1,0:T(8,128)(2,1)} %pad_maximum_fusion), calls=%async_computation | async-start | bytes 2097152 | tf_op jit(solution)/shard_map/all_to_all | solution.py:17
  77.0 146.4 %all-to-all-start.1 = ((bf16[32,24,2048]{2,1,0:T(8,128)(2,1)}), bf16[32,24,2048]{2,1,0:T(8,128)(2,1)}, u32[]{:S(2)}, u32[]{:S(2)}) async-start(bf16[32,24,2048]{2,1,0:T(8,128)(2,1)} %bitcast.52), calls=%async_computation.1 | async-start | bytes 6291456 | tf_op jit(solution)/shard_map/all_to_all | solution.py:93
  82.0 147.1 %copy-start.1 = (bf16[1,2048,128]{2,1,0:T(8,128)(2,1)}, bf16[1,2048,128]{2,1,0:T(8,128)(2,1)S(1)}, u32[]{:S(2)}) copy-start(bf16[1,2048,128]{2,1,0:T(8,128)(2,1)S(1)} %get-tuple-element.4) | copy-start | bytes 1572868
  82.0 147.1 %copy-start.3 = (bf16[1,2048,128]{2,1,0:T(8,128)(2,1)}, bf16[1,2048,128]{2,1,0:T(8,128)(2,1)S(1)}, u32[]{:S(2)}) copy-start(bf16[1,2048,128]{2,1,0:T(8,128)(2,1)S(1)} %get-tuple-element.3) | copy-start | bytes 1572868
  272.1 19.0 %copy-start.5 = (f32[128,4]{0,1:T(4,128)S(1)}, f32[128,4]{0,1:T(4,128)}, u32[]{:S(2)}) copy-start(f32[128,4]{0,1:T(4,128)} %param.9) | copy-start | bytes 6148
  285.1 18.4 %all-to-all-start.4 = ((bf16[16,2,1,24,128]{4,3,1,2,0:T(8,128)(2,1)}), bf16[16,2,1,24,128]{4,3,1,2,0:T(8,128)(2,1)S(1)}, u32[]{:S(2)}, u32[]{:S(2)}) async-start(bf16[16,2,1,24,128]{4,3,1,2,0:T(8,128)(2,1)} %copy.30), calls=%async_computation.4 | async-start | bytes 393216 | tf_op jit(solution)/shard_map/all_to_all | solution.py:49
where the time goes:
time: 309 us; the launch traced here: 305 us
  waiting for transfers between devices  200 us (65%)
  blocking collectives  51.1 us (17%)
  starting transfers between devices  27.6 us (9%)
  local copies, waits for them, and re-layouts  11.1 us (4%)
  other arithmetic  7.63 us (2%)
  matrix products  6.75 us (2%)
    all_to_all x1, waiting for transfers between devices, on_device(): lax.all_to_all(sender, FS, split_axis=0, concat_axis=0, tiled=True)  141 us
    all_to_all x1, waiting for transfers between devices, in_one_piece(): lax.all_to_all(both, axis, split_axis=split_dim, concat_axis=concat_dim,...  46.7 us
    all_to_all x1, blocking collectives, summed_on_arrival(): lax.all_to_all(in_blocks(shard, dim, peers), axis, 0, 0, tiled=True)  41.1 us
    all_to_all x1, starting transfers between devices, in_one_piece(): lax.all_to_all(both, axis, split_axis=split_dim, concat_axis=concat_dim,...  16.7 us
    all_to_all x1, waiting for transfers between devices, exchange_in_order(): filled = lax.all_to_all(filled, axes[k], k, k, tiled=True)  12.2 us
    all_to_all x1, blocking collectives, exchange_in_order(): filled = lax.all_to_all(filled, axes[k], k, k, tiled=True)  9.97 us
  transfers between devices with their start and end apart: 3, of which 3 were waited for; matrix products, arithmetic and copies ran while one was open for 3% of the time, Pallas kernels for 0%

commit v1 on v0

v1 whole, which is shorter than its diff:
```python
import jax
import jax.numpy as jnp
from jax import lax
from jax.sharding import PartitionSpec as P

clamp_limit = 7.0
gate_slope = 1.702
BF = jnp.bfloat16
F32 = jnp.float32


def dispatch_table(experts, routing, expert_count, capacity):
    tok = experts.shape[0]
    ids = experts.T
    names = jnp.arange(expert_count, dtype=jnp.int32)[:, None]
    chosen = jnp.zeros((expert_count, tok), F32)
    weight = jnp.zeros((expert_count, tok), F32)
    rt = routing.T
    for k in range(ids.shape[0]):
        hit = ids[k][None, :] == names
        chosen = chosen + jnp.where(hit, 1.0, 0.0)
        weight = weight + jnp.where(hit, rt[k][None, :], 0.0)
    before = (
        lax.broadcasted_iota(jnp.int32, (tok, tok), 0)
        < lax.broadcasted_iota(jnp.int32, (tok, tok), 1)
    ).astype(BF)
    rank = jnp.dot(chosen.astype(BF), before, preferred_element_type=F32)
    slot = jnp.where(chosen > 0, rank, -1.0)
    places = jnp.arange(capacity, dtype=jnp.int32).astype(F32)
    table = slot[:, None, :] == places[None, :, None]
    return table, weight


def on_device(tokens, experts, routing, norm_gain, gate_master, linear_master, down_weight):
    tok, top = experts.shape
    ecount, stripe, hid = gate_master.shape
    width = tokens.shape[1]
    n_tp = lax.axis_size("tp")
    fcols = width // n_tp
    cap = 3 * tok * top // (2 * ecount)
    gain = lax.dynamic_slice_in_dim(norm_gain, lax.axis_index("fs") * stripe, stripe)[None, :, None]
    both = jnp.concatenate(
        [(gate_master * gain).astype(BF), (linear_master * gain).astype(BF)], axis=2
    )
    filled = lax.all_to_all(both, "fs", split_axis=0, concat_axis=1, tiled=True)
    gate_out, linear_out = filled[:, :, :hid], filled[:, :, hid:]
    table, weight = dispatch_table(experts, routing, ecount, cap)
    pick = jnp.where(table, 1.0, 0.0).astype(BF).reshape(ecount * cap, tok)
    mine = lax.dynamic_slice_in_dim(tokens, lax.axis_index("tp") * fcols, fcols, axis=1)
    send = jnp.dot(pick, mine, preferred_element_type=F32).astype(BF)
    rows = lax.all_to_all(
        send.reshape(ecount, cap, fcols), "fs", split_axis=0, concat_axis=0, tiled=True
    )
    tokens_all = lax.all_gather(rows.reshape(ecount * cap, fcols), "tp", axis=0)
    down_mine = lax.all_to_all(
        down_weight[0].reshape(n_tp, fcols, hid), "tp", split_axis=0, concat_axis=0, tiled=True
    )
    dims = (((0, 2), (0, 1)), ((), ()))
    pre_gate = lax.dot_general(
        tokens_all, gate_out[0].reshape(n_tp, fcols, hid), dims, preferred_element_type=F32
    )
    pre_linear = lax.dot_general(
        tokens_all, linear_out[0].reshape(n_tp, fcols, hid), dims, preferred_element_type=F32
    )
    clamped = jnp.minimum(pre_gate, clamp_limit)
    active = (
        clamped
        * jax.nn.sigmoid(gate_slope * clamped)
        * (jnp.clip(pre_linear, -clamp_limit, clamp_limit) + 1.0)
    ).astype(BF)
    active_all = lax.all_gather(active, "tp", axis=0)
    summed = lax.dot_general(
        active_all, down_mine, (((0, 2), (0, 2)), ((), ())), preferred_element_type=F32
    )
    back = lax.all_to_all(
        summed.astype(BF).reshape(ecount, cap, fcols), "fs", split_axis=0, concat_axis=0, tiled=True
    ).reshape(ecount * cap, fcols)
    mixer = jnp.where(table, weight[:, None, :], 0.0).reshape(ecount * cap, tok)
    high = mixer.astype(BF)
    low = (mixer - high.astype(F32)).astype(BF)
    cdims = (((0,), (0,)), ((), ()))
    mix = lax.dot_general(high, back, cdims, preferred_element_type=F32) + lax.dot_general(
        low, back, cdims, preferred_element_type=F32
    )
    return gate_out, linear_out, mix.astype(BF)


def solution(mesh):
    return jax.shard_map(
        on_device,
        mesh=mesh,
        in_specs=(
            P("fs", None),
            P("fs", None),
            P("fs", None),
            P(),
            P(None, "fs", "tp"),
            P(None, "fs", "tp"),
            P("fs", None, "tp"),
        ),
        out_specs=(P("fs", None, "tp"), P("fs", None, "tp"), P("fs", "tp")),
        check_vma=False,
    )
```

time: 309 us -> 211 us (0.68)
  waiting for transfers between devices: 200 us -> 55.4 us
  blocking collectives: 51.1 us -> 113 us
  starting transfers between devices: 27.6 us -> 13.7 us
  between operations: 0.87 us -> 14.2 us
  local copies, waits for them, and re-layouts: 11.1 us -> 1.8 us
  other arithmetic: 7.63 us -> 2.21 us
  matrix products: 6.75 us -> 10.1 us
    all_to_all x3 -> x1, waiting for transfers between devices: 200 us -> 18.7 us  [on_device(): lax.all_to_all(summed.astype(BF).reshape(ecount, cap, fcols), 'fs', split...]
    all_to_all x2 -> x3, blocking collectives: 51.1 us -> 113 us  [the longest x1 59.9 us: on_device(): filled = lax.all_to_all(both, 'fs', split_axis=0, concat_axis=1, tiled=True)]
    all_gather x0 -> x2, waiting for transfers between devices: none -> 36.6 us  [the longest x1 36.6 us: on_device(): active_all = lax.all_gather(active, 'tp', axis=0)]
    all_to_all x3 -> x1, starting transfers between devices: 27.6 us -> 13.6 us  [on_device(): lax.all_to_all(summed.astype(BF).reshape(ecount, cap, fcols), 'fs', split...]
    gather x2 -> x0, local copies, waits for them, and re-layouts: 5.31 us -> none  [the longest x1 4.27 us: on_device(): sender = padded[slot_token].reshape(expert_count, capacity, width)]
    reduce_sum x3 -> x0, other arithmetic: 3.32 us -> none  [the longest x1 2.36 us: summed_on_arrival(): return jnp.sum(blocks.astype(jnp.float32), axis=0)]
    dot_general x3 -> x7, matrix products: 6.75 us -> 10.1 us  [the longest x1 3.55 us: on_device(): lax.dot_general(active_all, down_mine, (((0, 2), (0, 2)), ((), ())), pref...]
  transfers between devices with their start and end apart: 3 -> 3, of which waited for: 3 -> 2; matrix products, arithmetic and copies ran while one was open for 3% -> 1% of each run, Pallas kernels for 0% -> 0%
where the time goes in v1:
time: 211 us; the launch traced here: 210 us
  blocking collectives  113 us (54%)
  waiting for transfers between devices  55.4 us (26%)
  between operations  14.2 us (7%)
  starting transfers between devices  13.7 us (6%)
  matrix products  10.1 us (5%)
  other arithmetic  2.21 us (1%)
    all_to_all x1, blocking collectives, on_device(): filled = lax.all_to_all(both, 'fs', split_axis=0, concat_axis=1, tiled=True)  59.9 us
    all_gather x1, waiting for transfers between devices, on_device(): active_all = lax.all_gather(active, 'tp', axis=0)  36.6 us
    all_to_all x1, blocking collectives, on_device(): lax.all_to_all(send.reshape(ecount, cap, fcols), 'fs', split_axis=0, conc...  35.4 us
    all_to_all x1, waiting for transfers between devices, on_device(): lax.all_to_all(summed.astype(BF).reshape(ecount, cap, fcols), 'fs', split...  18.7 us
    all_to_all x1, blocking collectives, on_device(): lax.all_to_all(down_weight[0].reshape(n_tp, fcols, hid), 'tp', split_axis...  17.7 us
    all_to_all x1, starting transfers between devices, on_device(): lax.all_to_all(summed.astype(BF).reshape(ecount, cap, fcols), 'fs', split...  13.6 us
  transfers between devices with their start and end apart: 3, of which 2 were waited for; matrix products, arithmetic and copies ran while one was open for 1% of the time, Pallas kernels for 0%

profile of v1, /device:TPU:1, one launch (start us, length us, event | category | flops | bytes accessed | tf_op | source)
XLA Modules:
  0.0 210.4 jit_solution(13104925369870433439)
XLA Ops:
  7.2 0.0 all-gather.4.cloned.1.call-start
  7.2 0.8 slice_bitcast_fusion.7
  8.1 0.1 eq.124
  8.2 0.1 convolution_select_fusion
  8.3 0.2 select_convert_fusion.1
  8.5 0.2 convolution_convert_fusion
  8.7 35.4 %all_to_all.27 = bf16[32,24,128]{2,1,0:T(8,128)(2,1)} all-to-all(bf16[32,24,128]{2,1,0:T(8,128)(2,1)S(1)} %bitcast.66), channel_id=1, replica_groups=mesh['fs'=32,'tp'=16] {'fs'}, dimensions={0} | all-to-all | bytes 393216 | tf_op jit(solution)/shard_map/all_to_all | solution.py:51
  44.2 0.0 all-gather.6.cloned.1.call-start
  44.2 0.8 dynamic_slice.6
  45.0 1.9 multiply_convert_fusion.1
  46.9 0.1 pad_maximum_fusion
  47.0 59.9 %all_to_all.28 = bf16[32,64,256]{2,1,0:T(8,128)(2,1)S(1)} all-to-all(bf16[32,64,256]{2,1,0:T(8,128)(2,1)S(1)} %pad_maximum_fusion), channel_id=1, replica_groups=mesh['fs'=32,'tp'=16] {'fs'}, dimensions={0} | all-to-all | bytes 2097152 | tf_op jit(solution)/shard_map/all_to_all | solution.py:45
  106.9 0.1 fusion.34
  107.0 0.0 all-gather.4.cloned.1.call-done
  107.0 3.2 %fusion.3 = f32[768,128]{1,0:T(8,128)S(1)} fusion(bf16[16,768,128]{2,1,0:T(8,128)(2,1)} %all-gather.4.cloned.1.call-done, bf16[16,128,128]{2,1,0:T(8,128)(2,1)S(1)} %bitcast.64), kind=kOutput, calls=%fused_computation.6 | convolution fusion | flops 402751488 | bytes 4063232 | tf_op jit(solution)/shard_map/dot_general | solution.py:59
  110.3 1.7 fusion.4
  112.0 0.0 all-gather.6.cloned.1.call-update
  112.0 17.7 %all_to_all.29 = bf16[16,128,128]{2,1,0:T(8,128)(2,1)S(1)} all-to-all(bf16[16,128,128]{2,1,0:T(8,128)(2,1)S(1)} %bitcast.67), channel_id=1, replica_groups=mesh['fs'=32,'tp'=16] {'tp'}, dimensions={0} | all-to-all | bytes 1048576 | tf_op jit(solution)/shard_map/all_to_all | solution.py:55
  129.8 36.6 %all-gather.6.cloned.1.call-done = bf16[12288,128]{1,0:T(8,128)(2,1)} async-done(((bf16[768,128]{1,0:T(8,128)(2,1)}), bf16[12288,128]{1,0:T(8,128)(2,1)}) %all-gather.6.cloned.1.call-update) | async-done | bytes 3145744 | tf_op jit(solution)/shard_map/all_gather | solution.py:71
  166.3 3.5 %fusion.5 = bf16[768,128]{1,0:T(8,128)(2,1)} fusion(bf16[16,768,128]{2,1,0:T(8,128)(2,1)} %bitcast.71, bf16[16,128,128]{2,1,0:T(8,128)(2,1)S(1)} %all_to_all.29), kind=kOutput, calls=%fused_computation.9 | convolution fusion | flops 402751488 | bytes 3866624 | tf_op jit(solution)/shard_map/dot_general | solution.py:72
  169.9 13.6 %all-to-all-start.3 = ((bf16[32,24,128]{2,1,0:T(8,128)(2,1)}), bf16[32,24,128]{2,1,0:T(8,128)(2,1)S(1)}, u32[]{:S(2)}, u32[]{:S(2)}) async-start(bf16[32,24,128]{2,1,0:T(8,128)(2,1)} %bitcast.21), calls=%async_computation.3 | async-start | bytes 393216 | tf_op jit(solution)/shard_map/all_to_all | solution.py:75
  183.6 18.7 %all-to-all-done.3 = bf16[32,24,128]{2,1,0:T(8,128)(2,1)S(1)} async-done(((bf16[32,24,128]{2,1,0:T(8,128)(2,1)}), bf16[32,24,128]{2,1,0:T(8,128)(2,1)S(1)}, u32[]{:S(2)}, u32[]{:S(2)}) %all-to-all-start.3) | async-done | bytes 196640 | tf_op jit(solution)/shard_map/all_to_all | solution.py:75
  202.3 0.3 convolution_bitcast_fusion.3
  202.6 0.9 fusion.7
  (17 shorter events, 0.1 us)
Async XLA Ops:
  7.2 1.3 copy-start
  7.2 99.8 %all-gather.4.cloned.1.call-start = ((), (), s32[]{:S(2)}) async-start(), calls=%async_computation.4 | async-start | bytes 3342336 | tf_op jit(solution)/shard_map/all_gather | solution.py:54
  44.2 122.2 %all-gather.6.cloned.1.call-start = ((), (), s32[]{:S(2)}) async-start(), calls=%async_computation.5 | async-start | bytes 3342336 | tf_op jit(solution)/shard_map/all_gather | solution.py:71
  107.0 5.0 %copy-start.2 = (bf16[1,2048,128]{2,1,0:T(8,128)(2,1)}, bf16[1,2048,128]{2,1,0:T(8,128)(2,1)S(1)}, u32[]{:S(2)}) copy-start(bf16[1,2048,128]{2,1,0:T(8,128)(2,1)S(1)} %get-tuple-element.4) | copy-start | bytes 1572868
  107.0 5.0 %copy-start.4 = (bf16[1,2048,128]{2,1,0:T(8,128)(2,1)}, bf16[1,2048,128]{2,1,0:T(8,128)(2,1)S(1)}, u32[]{:S(2)}) copy-start(bf16[1,2048,128]{2,1,0:T(8,128)(2,1)S(1)} %get-tuple-element.3) | copy-start | bytes 1572868
  107.0 3.3 %copy-start.1 = (bf16[16,768,128]{2,1,0:T(8,128)(2,1)S(1)}, bf16[16,768,128]{2,1,0:T(8,128)(2,1)}, u32[]{:S(2)}) copy-start(bf16[16,768,128]{2,1,0:T(8,128)(2,1)} %all-gather.4.cloned.1.call-done) | copy-start | bytes 9437188
  110.3 1.7 copy-start.3
  112.0 71.5 %copy-start.5 = (f32[128,4]{0,1:T(4,128)S(1)}, f32[128,4]{0,1:T(4,128)}, u32[]{:S(2)}) copy-start(f32[128,4]{0,1:T(4,128)} %param.9) | copy-start | bytes 6148
  169.9 32.4 %all-to-all-start.3 = ((bf16[32,24,128]{2,1,0:T(8,128)(2,1)}), bf16[32,24,128]{2,1,0:T(8,128)(2,1)S(1)}, u32[]{:S(2)}, u32[]{:S(2)}) async-start(bf16[32,24,128]{2,1,0:T(8,128)(2,1)} %bitcast.21), calls=%async_computation.3 | async-start | bytes 393216 | tf_op jit(solution)/shard_map/all_to_all | solution.py:75
Sparse Core Ops, SparseCore 0:
  44.3 54.4 all-gather.3
  112.1 54.1 all-gather.5

commit v2 on v1

v2 whole, which is shorter than its diff:
```python
import functools

import jax
import jax.numpy as jnp
from jax import lax
from jax.experimental import pallas as pl
from jax.experimental.pallas import tpu as pltpu
from jax.sharding import PartitionSpec as P

clamp_limit = 7.0
gate_slope = 1.702
BF = jnp.bfloat16
F32 = jnp.float32
MESH = pl.DeviceIdType.MESH
SIDE = 4


def remote(src, dst, send_sem, recv_sem, device):
    return pltpu.make_async_remote_copy(
        src_ref=src,
        dst_ref=dst,
        send_sem=send_sem,
        recv_sem=recv_sem,
        device_id=device,
        device_id_type=MESH,
    )


class Torus:
    def __init__(self, grid, send_sems, recv_sems, t):
        self.grid, self.send_sems, self.recv_sems = grid, send_sems, recv_sems
        self.y, self.x = t // SIDE, t % SIDE
        tiles = grid.shape[1]
        self.half, self.quarter = tiles // 2, tiles // 4
        self.sent = []

    def at(self, h, a, b):
        dx, dy = (a, b) if h == 0 else (b, a)
        return ((self.y + dy + SIDE) % SIDE) * SIDE + (self.x + dx + SIDE) % SIDE

    def copy(self, h, slot, a, b, part, to):
        start = h * self.half + (self.quarter if part == 1 else 0)
        size = self.half if part is None else self.quarter
        ref = self.grid.at[self.at(h, a, b), pl.ds(start, size)]
        k = h * 20 + slot
        return remote(ref, ref, self.send_sems.at[k], self.recv_sems.at[k], {"tp": self.at(h, *to)})

    def send(self, h, slot, a, b, part, to):
        c = self.copy(h, slot, a, b, part, to)
        c.start()
        self.sent.append(c)

    def recv(self, h, slot, a, b, part):
        self.copy(h, slot, a, b, part, (1, 0)).wait_recv()

    def own(self):
        for h in (0, 1):
            self.send(h, 0, 0, 0, None, (1, 0))
            self.send(h, 1, 0, 0, None, (-1, 0))
            self.column(h, 0, 0)

    def column(self, h, i, a):
        self.send(h, 4 + 4 * i, a, 0, None, (0, 1))
        self.send(h, 5 + 4 * i, a, 0, None, (0, -1))

    def turn(self, h, i, a):
        self.recv(h, 4 + 4 * i, a, -1, None)
        self.send(h, 6 + 4 * i, a, -1, 0, (0, 1))
        self.recv(h, 5 + 4 * i, a, 1, None)
        self.send(h, 7 + 4 * i, a, 1, 1, (0, -1))

    def rest(self):
        for h in (0, 1):
            self.recv(h, 0, -1, 0, None)
            self.send(h, 2, -1, 0, 0, (1, 0))
            self.column(h, 1, -1)
            self.recv(h, 1, 1, 0, None)
            self.send(h, 3, 1, 0, 1, (-1, 0))
            self.column(h, 2, 1)
        for h in (0, 1):
            self.turn(h, 0, 0)
        for h in (0, 1):
            self.recv(h, 2, 2, 0, 0)
            self.recv(h, 3, 2, 0, 1)
            self.column(h, 3, 2)
        for h in (0, 1):
            self.turn(h, 1, -1)
            self.turn(h, 2, 1)
        for h in (0, 1):
            self.turn(h, 3, 2)
        for h in (0, 1):
            for i, a in enumerate((0, -1, 1, 2)):
                self.recv(h, 6 + 4 * i, a, 2, 0)
                self.recv(h, 7 + 4 * i, a, 2, 1)

    def drain(self):
        for c in self.sent:
            c.wait_send()


def kernel(
    n_fs,
    n_tp,
    experts_ref,
    routing_ref,
    gain_ref,
    tokens_hbm,
    gate_hbm,
    linear_hbm,
    down_hbm,
    gate_out,
    linear_out,
    mix_out,
    gate_v,
    linear_v,
    tok_v,
    down_v,
    w_send,
    w_recv,
    t_send,
    t_grid,
    a_grid,
    d_recv,
    r_send,
    r_recv,
    slot_v,
    weight_v,
    pick_v,
    mixer_v,
    high_v,
    low_v,
    acc,
    acc2,
    local_sems,
    t_ssem,
    t_rsem,
    w_ssem,
    w_rsem,
    r_ssem,
    r_rsem,
    d_ssem,
    d_rsem,
    tg_ssem,
    tg_rsem,
    ag_ssem,
    ag_rsem,
):
    f, t = lax.axis_index("fs"), lax.axis_index("tp")
    n_z = n_fs // 2
    z, c = f // 2, f % 2
    stripe, hid = gate_v.shape[1], gate_v.shape[2]
    fcols = tok_v.shape[1]
    tok = tok_v.shape[0]
    tiles = t_grid.shape[1]
    rows = tiles * 8
    per = tiles // n_fs
    cap = per * 8

    loads = [
        pltpu.make_async_copy(
            tokens_hbm.at[:, pl.ds(pl.multiple_of(t * fcols, 128), fcols)], tok_v, local_sems.at[0]
        ),
        pltpu.make_async_copy(gate_hbm, gate_v, local_sems.at[1]),
        pltpu.make_async_copy(linear_hbm, linear_v, local_sems.at[2]),
        pltpu.make_async_copy(down_hbm, down_v, local_sems.at[3]),
    ]
    for load in loads:
        load.start()

    barrier = pltpu.get_barrier_semaphore()

    @pl.loop(1, n_fs)
    def _(k):
        pl.semaphore_signal(
            barrier, inc=1, device_id={"fs": (f + k) % n_fs}, device_id_type=MESH
        )

    @pl.loop(1, n_tp)
    def _(k):
        pl.semaphore_signal(
            barrier, inc=1, device_id={"tp": (t + k) % n_tp}, device_id_type=MESH
        )

    names = lax.broadcasted_iota(jnp.int32, (n_fs, tok), 0)
    chosen = jnp.zeros((n_fs, tok), F32)
    weight = jnp.zeros((n_fs, tok), F32)
    for k in range(experts_ref.shape[0]):
        hit = experts_ref[k : k + 1, :] == names
        chosen = chosen + jnp.where(hit, 1.0, 0.0)
        weight = weight + jnp.where(hit, routing_ref[k : k + 1, :], 0.0)
    before = jnp.where(
        lax.broadcasted_iota(jnp.int32, (tok, tok), 0)
        < lax.broadcasted_iota(jnp.int32, (tok, tok), 1),
        1.0,
        0.0,
    ).astype(BF)
    rank = jnp.dot(chosen.astype(BF), before, preferred_element_type=F32)
    slot_v[...] = jnp.where(chosen > 0.0, rank, -1.0)
    weight_v[...] = weight
    places = lax.broadcasted_iota(jnp.int32, (cap, tok), 0).astype(F32)

    @pl.loop(0, n_fs)
    def _(e):
        hit = slot_v[pl.ds(e, 1), :] == places
        at = pl.ds(pl.multiple_of(e * cap, 8), cap)
        pick_v[at, :] = jnp.where(hit, 1.0, 0.0)
        mixer_v[at, :] = jnp.where(hit, weight_v[pl.ds(e, 1), :], 0.0)

    loads[0].wait()
    sent = jnp.dot(pick_v[...].astype(BF), tok_v[...], preferred_element_type=F32)
    t_send[...] = sent.astype(BF).reshape(tiles, 8, fcols)

    here = lax.broadcasted_iota(jnp.int32, (stripe, hid), 0) + (f * stripe) % hid
    lane = lax.broadcasted_iota(jnp.int32, (stripe, hid), 1)
    picked = jnp.where(here == lane, gain_ref[pl.ds((f * stripe) // hid, 1), :], 0.0)
    column = jnp.sum(picked, axis=1, keepdims=True)
    loads[1].wait()
    loads[2].wait()

    @pl.loop(0, n_fs)
    def _(e):
        w_send[e, :, 0:hid] = (gate_v[e] * column).astype(BF)
        w_send[e, :, hid : 2 * hid] = (linear_v[e] * column).astype(BF)

    loads[3].wait()
    pl.semaphore_wait(barrier, n_fs + n_tp - 2)

    def tile_span(i):
        return pl.ds(i * per, per)

    def peer(dz, dc):
        return ((z + dz) % n_z) * 2 + (c + dc) % 2

    def source(dz, dc):
        return ((z - dz + n_z) % n_z) * 2 + (c + dc) % 2

    def turn(k):
        return (n_z // 2 + (1 - 2 * (k % 2)) * ((k + 1) // 2)) % n_z

    def tokens_copy(dz, dc, to, slot):
        i = dz * 2 + dc
        return remote(
            t_send.at[tile_span(to)],
            t_grid.at[t, tile_span(slot)],
            t_ssem.at[i],
            t_rsem.at[i],
            {"fs": to},
        )

    def weights_copy(dz, dc, to, slot):
        i = dz * 2 + dc
        return remote(w_send.at[to], w_recv.at[slot], w_ssem.at[i], w_rsem.at[i], {"fs": to})

    def return_copy(dz, dc, to, slot):
        i = dz * 2 + dc
        return remote(
            r_send.at[tile_span(to)],
            r_recv.at[tile_span(slot)],
            r_ssem.at[i],
            r_rsem.at[i],
            {"fs": to},
        )

    def start_all(copy):
        @pl.loop(0, n_z - 1)
        def _(k):
            dz = turn(k)
            for dc in (0, 1):
                copy(dz, dc, peer(dz, dc), f).start()

        copy(0, 1, peer(0, 1), f).start()

    def recv_all(copy):
        copy(0, 1, peer(0, 1), source(0, 1)).wait_recv()

        @pl.loop(0, n_z - 1)
        def _(k):
            dz = turn(k)
            for dc in (0, 1):
                copy(dz, dc, peer(dz, dc), source(dz, dc)).wait_recv()

    def drain_all(copy):
        copy(0, 1, peer(0, 1), f).wait_send()

        @pl.loop(0, n_z - 1)
        def _(k):
            dz = turn(k)
            for dc in (0, 1):
                copy(dz, dc, peer(dz, dc), f).wait_send()

    def down_copy(k, slot):
        to = (t + k) % n_tp
        return remote(
            down_v.at[to], d_recv.at[slot], d_ssem.at[k], d_rsem.at[k], {"tp": to}
        )

    start_all(tokens_copy)
    start_all(weights_copy)

    @pl.loop(1, n_tp)
    def _(k):
        down_copy(k, t).start()

    t_grid[t, tile_span(f)] = t_send[tile_span(f)]
    w_recv[f] = w_send[f]
    d_recv[t] = down_v[t]
    for j in range(rows // 128):
        at = slice(j * 128, (j + 1) * 128)
        turned = mixer_v[at, :].T
        high = turned.astype(BF)
        high_v[:, at] = high
        low_v[:, at] = (turned - high.astype(F32)).astype(BF)
    acc[...] = jnp.zeros_like(acc)

    recv_all(tokens_copy)
    tg = Torus(t_grid, tg_ssem, tg_rsem, t)
    tg.own()
    tg.rest()

    ratio = (2 * stripe) // fcols

    def multiply(chip):
        for j in range(ratio):
            block = chip * ratio + j
            lhs = t_grid[block].reshape(rows, fcols)
            if ratio == 1:
                rhs = w_recv[pl.ds(chip * 2, 2)].reshape(fcols, 2 * hid)
            else:
                rhs = w_recv[chip * 2 + j // (ratio // 2), (j % (ratio // 2)) * fcols :][:fcols]
            acc[...] += jnp.dot(lhs, rhs, preferred_element_type=F32)

    weights_copy(0, 1, peer(0, 1), source(0, 1)).wait_recv()
    multiply(z)

    @pl.loop(0, n_z - 1)
    def _(k):
        dz = turn(k)
        for dc in (0, 1):
            weights_copy(dz, dc, peer(dz, dc), source(dz, dc)).wait_recv()
        multiply((z - dz + n_z) % n_z)

    stores = [
        pltpu.make_async_copy(w_recv.at[:, :, pl.ds(0, hid)], gate_out, local_sems.at[4]),
        pltpu.make_async_copy(w_recv.at[:, :, pl.ds(hid, hid)], linear_out, local_sems.at[5]),
    ]
    for store in stores:
        store.start()

    clamped = jnp.minimum(acc[:, 0:hid], clamp_limit)
    linear = jnp.clip(acc[:, hid : 2 * hid], -clamp_limit, clamp_limit)
    active = clamped * jax.nn.sigmoid(gate_slope * clamped) * (linear + 1.0)
    a_grid[t] = active.astype(BF).reshape(tiles, 8, hid)

    ag = Torus(a_grid, ag_ssem, ag_rsem, t)
    ag.own()
    acc2[...] = jnp.zeros_like(acc2)

    @pl.loop(1, n_tp)
    def _(k):
        down_copy(k, (t - k + n_tp) % n_tp).wait_recv()

    ag.rest()

    @pl.loop(0, n_tp)
    def _(b):
        acc2[...] += lax.dot_general(
            a_grid[b].reshape(rows, hid),
            d_recv[b],
            (((1,), (1,)), ((), ())),
            preferred_element_type=F32,
        )

    r_send[...] = acc2[...].astype(BF).reshape(tiles, 8, fcols)
    start_all(return_copy)
    r_recv[tile_span(f)] = r_send[tile_span(f)]
    drain_all(tokens_copy)
    drain_all(weights_copy)

    @pl.loop(1, n_tp)
    def _(k):
        down_copy(k, t).wait_send()

    tg.drain()
    ag.drain()
    for store in stores:
        store.wait()
    recv_all(return_copy)
    back = r_recv[...].reshape(rows, fcols)
    mix = jnp.dot(high_v[...], back, preferred_element_type=F32) + jnp.dot(
        low_v[...], back, preferred_element_type=F32
    )
    mix_out[...] = mix.astype(BF)
    drain_all(return_copy)


def on_device(n_fs, n_tp, tokens, experts, routing, gain, gate_master, linear_master, down_weight):
    tok, top = experts.shape
    ecount, stripe, hid = gate_master.shape
    width = tokens.shape[1]
    fcols = width // n_tp
    cap = 3 * tok * top // (2 * ecount)
    tiles = ecount * cap // 8
    rows = ecount * cap
    vmem, any_space = pl.BlockSpec(memory_space=pltpu.VMEM), pl.BlockSpec(memory_space=pl.ANY)
    dma = pltpu.SemaphoreType.DMA
    gate_out, linear_out, mix = pl.pallas_call(
        functools.partial(kernel, n_fs, n_tp),
        out_shape=(
            jax.ShapeDtypeStruct((ecount, stripe, hid), BF),
            jax.ShapeDtypeStruct((ecount, stripe, hid), BF),
            jax.ShapeDtypeStruct((tok, fcols), BF),
        ),
        in_specs=[vmem] * 3 + [any_space] * 4,
        out_specs=(any_space, any_space, vmem),
        scratch_shapes=[
            pltpu.VMEM((ecount, stripe, hid), F32),
            pltpu.VMEM((ecount, stripe, hid), F32),
            pltpu.VMEM((tok, fcols), BF),
            pltpu.VMEM((n_tp, fcols, hid), BF),
            pltpu.VMEM((ecount, stripe, 2 * hid), BF),
            pltpu.VMEM((ecount, stripe, 2 * hid), BF),
            pltpu.VMEM((tiles, 8, fcols), BF),
            pltpu.VMEM((n_tp, tiles, 8, fcols), BF),
            pltpu.VMEM((n_tp, tiles, 8, hid), BF),
            pltpu.VMEM((n_tp, fcols, hid), BF),
            pltpu.VMEM((tiles, 8, fcols), BF),
            pltpu.VMEM((tiles, 8, fcols), BF),
            pltpu.VMEM((ecount, tok), F32),
            pltpu.VMEM((ecount, tok), F32),
            pltpu.VMEM((rows, tok), F32),
            pltpu.VMEM((rows, tok), F32),
            pltpu.VMEM((tok, rows), BF),
            pltpu.VMEM((tok, rows), BF),
            pltpu.VMEM((rows, 2 * hid), F32),
            pltpu.VMEM((rows, fcols), F32),
            dma((6,)),
            dma((n_fs,)),
            dma((n_fs,)),
            dma((n_fs,)),
            dma((n_fs,)),
            dma((n_fs,)),
            dma((n_fs,)),
            dma((n_tp,)),
            dma((n_tp,)),
            dma((40,)),
            dma((40,)),
            dma((40,)),
            dma((40,)),
        ],
        compiler_params=pltpu.CompilerParams(
            collective_id=0, has_side_effects=True, vmem_limit_bytes=48 * 1024 * 1024
        ),
    )(
        experts.T,
        routing.T,
        gain.reshape(width // hid, hid),
        tokens,
        gate_master,
        linear_master,
        down_weight.reshape(n_tp, fcols, hid),
    )
    shape = (1, width, hid)
    return gate_out.reshape(shape), linear_out.reshape(shape), mix


def solution(mesh):
    n_fs, n_tp = mesh.shape["fs"], mesh.shape["tp"]
    return jax.shard_map(
        functools.partial(on_device, n_fs, n_tp),
        mesh=mesh,
        in_specs=(
            P("fs", None),
            P("fs", None),
            P("fs", None),
            P(),
            P(None, "fs", "tp"),
            P(None, "fs", "tp"),
            P("fs", None, "tp"),
        ),
        out_specs=(P("fs", None, "tp"), P("fs", None, "tp"), P("fs", "tp")),
        check_vma=False,
    )
```

time: 211 us -> 121 us (0.57)
  blocking collectives: 113 us -> 0 us
  Pallas kernels: 0 us -> 112 us
  waiting for transfers between devices: 55.4 us -> 0 us
  starting transfers between devices: 13.7 us -> 0 us
  between operations: 14.2 us -> 0.66 us
  matrix products: 10.1 us -> 0 us
  local copies, waits for them, and re-layouts: 1.8 us -> 8.11 us
  other arithmetic: 2.21 us -> 0 us
    all_to_all x3 -> x0, blocking collectives: 113 us -> none  [the longest x1 59.9 us: on_device(): filled = lax.all_to_all(both, 'fs', split_axis=0, concat_axis=1, tiled=True)]
    pallas_call x0 -> x1, Pallas kernels: none -> 112 us  [on_device(): pl.pallas_call(functools.partial(kernel, n_fs, n_tp), out_shape=(jax.Shap...]
    all_gather x2 -> x0, waiting for transfers between devices: 36.6 us -> none  [the longest x1 36.6 us: on_device(): active_all = lax.all_gather(active, 'tp', axis=0)]
    all_to_all x1 -> x0, waiting for transfers between devices: 18.7 us -> none  [on_device(): lax.all_to_all(summed.astype(BF).reshape(ecount, cap, fcols), 'fs', split...]
    all_to_all x1 -> x0, starting transfers between devices: 13.6 us -> none  [on_device(): lax.all_to_all(summed.astype(BF).reshape(ecount, cap, fcols), 'fs', split...]
    dot_general x7 -> x0, matrix products: 10.1 us -> none  [the longest x1 3.55 us: on_device(): lax.dot_general(active_all, down_mine, (((0, 2), (0, 2)), ((), ())), pref...]
    unnamed x12 -> x17, local copies, waits for them, and re-layouts: 0.04 us -> 8.11 us
  transfers between devices with their start and end apart: 3 -> 0, of which waited for: 2 -> 0; matrix products, arithmetic and copies ran while one was open for 1% -> 0% of each run, Pallas kernels for 0% -> 0%
where the time goes in v2:
time: 121 us
  Pallas kernels  112 us (93%)
  local copies, waits for them, and re-layouts  8.11 us (7%)
    pallas_call x1, Pallas kernels, on_device(): pl.pallas_call(functools.partial(kernel, n_fs, n_tp), out_shape=(jax.Shap...  112 us
    unnamed x17, local copies, waits for them, and re-layouts  8.11 us

profile of v2, /device:TPU:1, one launch (start us, length us, event | category | flops | bytes accessed | tf_op | source)
XLA Modules:
  0.0 120.7 jit_solution(14192739054346763961)
XLA Ops:
  0.6 0.0 copy-start.6
  0.6 0.0 copy-start.5
  0.7 0.7 copy-done.6
  1.3 0.0 copy-done.5
  1.3 0.0 copy-start
  1.3 1.2 %copy-done = f32[32,64,128]{2,1,0:T(8,128)S(1)} copy-done((f32[32,64,128]{2,1,0:T(8,128)S(1)}, f32[32,64,128]{2,1,0:T(8,128)}, u32[]{:S(2)}) %copy-start) | copy-done | bytes 1048600
  2.6 0.0 copy-start.1
  2.6 1.2 %copy-done.1 = f32[32,64,128]{2,1,0:T(8,128)S(1)} copy-done((f32[32,64,128]{2,1,0:T(8,128)S(1)}, f32[32,64,128]{2,1,0:T(8,128)}, u32[]{:S(2)}) %copy-start.1) | copy-done | bytes 1048600
  3.8 0.0 copy-start.2
  3.8 1.0 copy-done.2
  4.8 0.0 copy-start.3
  4.8 1.0 copy-done.3
  5.9 0.0 copy-start.4
  5.9 0.7 copy-done.4
  6.6 111.9 %shard_map.94 = (bf16[32,64,128]{2,1,0:T(8,128)(2,1)S(1)}, bf16[32,64,128]{2,1,0:T(8,128)(2,1)S(1)}, bf16[128,128]{1,0:T(8,128)(2,1)S(1)}) custom-call(s32[4,128]{1,0:T(4,128)S(1)} %bitcast.10, f32[4,128]{1,0:T(4,128)S(1)} %bitcast.11, f32[16,128]{1,0:T(8,128)S(1)} %bitcast.9, bf16[128,2048]{1,0:T(8,128)(2,1)S(1)} %copy-done.2, f32[32,64,128]{2,1,0:T(8,128)S(1)} %copy-done, ...), custom_call_target="tpu_custom_call" | custom-call | tf_op jit(solution)/shard_map/pallas_call | solution.py:406
  118.5 0.8 copy.13
  119.3 0.8 copy.14
  120.1 0.6 copy.15
Async XLA Ops:
  0.6 0.7 copy-start.6
  0.6 0.7 copy-start.5
  1.3 1.2 %copy-start = (f32[32,64,128]{2,1,0:T(8,128)S(1)}, f32[32,64,128]{2,1,0:T(8,128)}, u32[]{:S(2)}) copy-start(f32[32,64,128]{2,1,0:T(8,128)} %gate_hbm.1) | copy-start | bytes 3145732
  2.6 1.2 %copy-start.1 = (f32[32,64,128]{2,1,0:T(8,128)S(1)}, f32[32,64,128]{2,1,0:T(8,128)}, u32[]{:S(2)}) copy-start(f32[32,64,128]{2,1,0:T(8,128)} %linear_hbm.1) | copy-start | bytes 3145732
  3.8 1.0 copy-start.2
  4.8 1.0 copy-start.3
  5.9 0.7 copy-start.4

commit v3 on v2

--- a/solution.py
+++ b/solution.py
@@ -98,12 +98,51 @@
             c.wait_send()
 
 
+class Ring:
+    def __init__(self, ref_of, device_of, send_sems, recv_sems, pos):
+        self.ref_of, self.device_of, self.pos = ref_of, device_of, pos
+        self.send_sems, self.recv_sems, self.sent = send_sems, recv_sems, []
+
+    def at(self, step):
+        return (self.pos + step + SIDE) % SIDE
+
+    def copy(self, item, slot, step, part, to):
+        ref = self.ref_of(self.at(step), item, part)
+        k = item * 4 + slot
+        return remote(
+            ref, ref, self.send_sems.at[k], self.recv_sems.at[k], self.device_of(self.at(to))
+        )
+
+    def send(self, item, slot, step, part, to):
+        c = self.copy(item, slot, step, part, to)
+        c.start()
+        self.sent.append(c)
+
+    def first(self, item):
+        self.send(item, 0, 0, None, 1)
+        self.send(item, 1, 0, None, -1)
+
+    def second(self, item):
+        self.copy(item, 0, -1, None, 1).wait_recv()
+        self.send(item, 2, -1, 0, 1)
+        self.copy(item, 1, 1, None, 1).wait_recv()
+        self.send(item, 3, 1, 1, -1)
+
+    def last(self, item):
+        self.copy(item, 2, 2, 0, 1).wait_recv()
+        self.copy(item, 3, 2, 1, 1).wait_recv()
+
+    def drain(self):
+        for c in self.sent:
+            c.wait_send()
+
+
 def kernel(
     n_fs,
     n_tp,
-    experts_ref,
-    routing_ref,
-    gain_ref,
+    experts_hbm,
+    routing_hbm,
+    gain_hbm,
     tokens_hbm,
     gate_hbm,
     linear_hbm,
@@ -111,6 +150,9 @@
     gate_out,
     linear_out,
     mix_out,
+    experts_ref,
+    routing_ref,
+    gain_ref,
     gate_v,
     linear_v,
     tok_v,
@@ -119,8 +161,9 @@
     w_recv,
     t_send,
     t_grid,
+    a_send,
     a_grid,
-    d_recv,
+    d_grid,
     r_send,
     r_recv,
     slot_v,
@@ -138,12 +181,16 @@
     w_rsem,
     r_ssem,
     r_rsem,
-    d_ssem,
-    d_rsem,
+    dy_ssem,
+    dy_rsem,
+    dx_ssem,
+    dx_rsem,
     tg_ssem,
     tg_rsem,
-    ag_ssem,
-    ag_rsem,
+    ax_ssem,
+    ax_rsem,
+    ay_ssem,
+    ay_rsem,
 ):
     f, t = lax.axis_index("fs"), lax.axis_index("tp")
     n_z = n_fs // 2
@@ -156,6 +203,7 @@
     per = tiles // n_fs
     cap = per * 8
 
+    y, x = t // SIDE, t % SIDE
     loads = [
         pltpu.make_async_copy(
             tokens_hbm.at[:, pl.ds(pl.multiple_of(t * fcols, 128), fcols)], tok_v, local_sems.at[0]
@@ -163,6 +211,9 @@
         pltpu.make_async_copy(gate_hbm, gate_v, local_sems.at[1]),
         pltpu.make_async_copy(linear_hbm, linear_v, local_sems.at[2]),
         pltpu.make_async_copy(down_hbm, down_v, local_sems.at[3]),
+        pltpu.make_async_copy(experts_hbm, experts_ref, local_sems.at[4]),
+        pltpu.make_async_copy(routing_hbm, routing_ref, local_sems.at[5]),
+        pltpu.make_async_copy(gain_hbm, gain_ref, local_sems.at[6]),
     ]
     for load in loads:
         load.start()
@@ -181,6 +232,8 @@
             barrier, inc=1, device_id={"tp": (t + k) % n_tp}, device_id_type=MESH
         )
 
+    loads[4].wait()
+    loads[5].wait()
     names = lax.broadcasted_iota(jnp.int32, (n_fs, tok), 0)
     chosen = jnp.zeros((n_fs, tok), F32)
     weight = jnp.zeros((n_fs, tok), F32)
@@ -210,6 +263,7 @@
     sent = jnp.dot(pick_v[...].astype(BF), tok_v[...], preferred_element_type=F32)
     t_send[...] = sent.astype(BF).reshape(tiles, 8, fcols)
 
+    loads[6].wait()
     here = lax.broadcasted_iota(jnp.int32, (stripe, hid), 0) + (f * stripe) % hid
     lane = lax.broadcasted_iota(jnp.int32, (stripe, hid), 1)
     picked = jnp.where(here == lane, gain_ref[pl.ds((f * stripe) // hid, 1), :], 0.0)
@@ -251,16 +305,6 @@
         i = dz * 2 + dc
         return remote(w_send.at[to], w_recv.at[slot], w_ssem.at[i], w_rsem.at[i], {"fs": to})
 
-    def return_copy(dz, dc, to, slot):
-        i = dz * 2 + dc
-        return remote(
-            r_send.at[tile_span(to)],
-            r_recv.at[tile_span(slot)],
-            r_ssem.at[i],
-            r_rsem.at[i],
-            {"fs": to},
-        )
-
     def start_all(copy):
         @pl.loop(0, n_z - 1)
         def _(k):
@@ -288,22 +332,29 @@
             for dc in (0, 1):
                 copy(dz, dc, peer(dz, dc), f).wait_send()
 
-    def down_copy(k, slot):
-        to = (t + k) % n_tp
+    def down_y(k, slot):
+        to = (y + k) % SIDE
         return remote(
-            down_v.at[to], d_recv.at[slot], d_ssem.at[k], d_rsem.at[k], {"tp": to}
+            down_v.at[to], d_grid.at[slot, x], dy_ssem.at[k], dy_rsem.at[k], {"tp": to * SIDE + x}
         )
+
+    def down_ref(p, k, part):
+        block = d_grid.at[(y - k + SIDE) % SIDE, p]
+        half = d_grid.shape[2] // 2
+        return block if part is None else block.at[pl.ds(part * half, half)]
+
+    dx = Ring(down_ref, lambda p: {"tp": y * SIDE + p}, dx_ssem, dx_rsem, x)
 
     start_all(tokens_copy)
     start_all(weights_copy)
 
-    @pl.loop(1, n_tp)
-    def _(k):
-        down_copy(k, t).start()
+    for k in (1, 3, 2):
+        down_y(k, y).start()
+    d_grid[y, x] = down_v[y]
+    dx.first(0)
 
     t_grid[t, tile_span(f)] = t_send[tile_span(f)]
     w_recv[f] = w_send[f]
-    d_recv[t] = down_v[t]
     for j in range(rows // 128):
         at = slice(j * 128, (j + 1) * 128)
         turned = mixer_v[at, :].T
@@ -312,9 +363,15 @@
         low_v[:, at] = (turned - high.astype(F32)).astype(BF)
     acc[...] = jnp.zeros_like(acc)
 
+    for k in (1, 3, 2):
+        down_y(k, (y - k + SIDE) % SIDE).wait_recv()
+        dx.first(k)
+
     recv_all(tokens_copy)
     tg = Torus(t_grid, tg_ssem, tg_rsem, t)
     tg.own()
+    for k in (0, 1, 3, 2):
+        dx.second(k)
     tg.rest()
 
     ratio = (2 * stripe) // fcols
@@ -340,8 +397,8 @@
         multiply((z - dz + n_z) % n_z)
 
     stores = [
-        pltpu.make_async_copy(w_recv.at[:, :, pl.ds(0, hid)], gate_out, local_sems.at[4]),
-        pltpu.make_async_copy(w_recv.at[:, :, pl.ds(hid, hid)], linear_out, local_sems.at[5]),
+        pltpu.make_async_copy(w_recv.at[:, :, pl.ds(0, hid)], gate_out, local_sems.at[7]),
+        pltpu.make_async_copy(w_recv.at[:, :, pl.ds(hid, hid)], linear_out, local_sems.at[8]),
     ]
     for store in stores:
         store.start()
@@ -349,48 +406,115 @@
     clamped = jnp.minimum(acc[:, 0:hid], clamp_limit)
     linear = jnp.clip(acc[:, hid : 2 * hid], -clamp_limit, clamp_limit)
     active = clamped * jax.nn.sigmoid(gate_slope * clamped) * (linear + 1.0)
-    a_grid[t] = active.astype(BF).reshape(tiles, 8, hid)
-
-    ag = Torus(a_grid, ag_ssem, ag_rsem, t)
-    ag.own()
+    a_send[...] = active.astype(BF).reshape(a_send.shape)
+
+    def active_x(k, slot):
+        to = (x + k) % SIDE
+        return remote(
+            a_send.at[:, to], a_grid.at[y, slot], ax_ssem.at[k], ax_rsem.at[k], {"tp": y * SIDE + to}
+        )
+
+    def active_ref(p, k, part):
+        block = a_grid.at[p, (x - k + SIDE) % SIDE]
+        half = a_grid.shape[2] // 2
+        return block if part is None else block.at[pl.ds(part * half, half)]
+
+    ay = Ring(active_ref, lambda p: {"tp": p * SIDE + x}, ay_ssem, ay_rsem, y)
+    groups = (1, 3, 2)
+    for k in groups:
+        active_x(k, x).start()
+    a_grid[y, x] = a_send[:, x]
+    ay.first(0)
     acc2[...] = jnp.zeros_like(acc2)
-
-    @pl.loop(1, n_tp)
-    def _(k):
-        down_copy(k, (t - k + n_tp) % n_tp).wait_recv()
-
-    ag.rest()
-
-    @pl.loop(0, n_tp)
-    def _(b):
+    share = acc2.shape[0]
+
+    def multiply_down(step, k):
+        p, g = (y + step + SIDE) % SIDE, (x - k + SIDE) % SIDE
         acc2[...] += lax.dot_general(
-            a_grid[b].reshape(rows, hid),
-            d_recv[b],
+            a_grid[p, g].reshape(share, hid),
+            d_grid[p, g],
             (((1,), (1,)), ((), ())),
             preferred_element_type=F32,
         )
 
-    r_send[...] = acc2[...].astype(BF).reshape(tiles, 8, fcols)
-    start_all(return_copy)
-    r_recv[tile_span(f)] = r_send[tile_span(f)]
+    for k in (0,) + groups:
+        dx.last(k)
+    multiply_down(0, 0)
+    for k in groups:
+        active_x(k, (x - k + SIDE) % SIDE).wait_recv()
+        ay.first(k)
+    for k in groups:
+        multiply_down(0, k)
+    for k in (0,) + groups:
+        ay.second(k)
+        multiply_down(-1, k)
+        multiply_down(1, k)
+    for k in (0,) + groups:
+        ay.last(k)
+        multiply_down(2, k)
+
+    for p in range(SIDE):
+        part = acc2[:, p * fcols : (p + 1) * fcols].astype(BF)
+        r_send[p] = part.reshape(r_send.shape[1:])
+
+    def return_copy(q, core, p):
+        chip = q * SIDE + x
+        to = chip * 2 + core
+        return remote(
+            r_send.at[p, q * 2 + core],
+            r_recv.at[f],
+            r_ssem.at[(q * 2 + core) * SIDE + p],
+            r_rsem.at[f],
+            {"fs": to, "tp": y * SIDE + p},
+        ), jnp.logical_and(to == f, p == x)
+
+    def each_return(act):
+        @pl.loop(0, n_z // SIDE)
+        def _(k):
+            q = (z // SIDE + n_z // SIDE // 2 + k) % (n_z // SIDE)
+            for core in (0, 1):
+                for p in range(SIDE):
+                    c, local = return_copy(q, core, p)
+
+                    @pl.when(jnp.logical_not(local))
+                    def _():
+                        act(c)
+
+    each_return(lambda c: c.start())
+
+    @pl.when(z % SIDE == x)
+    def _():
+        r_recv[f] = r_send[x, (z // SIDE) * 2 + c]
+
     drain_all(tokens_copy)
     drain_all(weights_copy)
-
-    @pl.loop(1, n_tp)
-    def _(k):
-        down_copy(k, t).wait_send()
-
+    for k in groups:
+        down_y(k, y).wait_send()
+        active_x(k, x).wait_send()
+    dx.drain()
     tg.drain()
-    ag.drain()
+    ay.drain()
     for store in stores:
         store.wait()
-    recv_all(return_copy)
+
+    @pl.loop(0, n_fs)
+    def _(e):
+        @pl.when(jnp.logical_not(jnp.logical_and(e == f, z % SIDE == x)))
+        def _():
+            remote(
+                r_send.at[0, 0],
+                r_recv.at[e],
+                r_ssem.at[0],
+                r_rsem.at[e],
+                {"fs": e, "tp": y * SIDE + z % SIDE},
+            ).wait_recv()
+
     back = r_recv[...].reshape(rows, fcols)
     mix = jnp.dot(high_v[...], back, preferred_element_type=F32) + jnp.dot(
         low_v[...], back, preferred_element_type=F32
     )
     mix_out[...] = mix.astype(BF)
-    drain_all(return_copy)
+    each_return(lambda c: c.wait_send())
 
 
 def on_device(n_fs, n_tp, tokens, experts, routing, gain, gate_master, linear_master, down_weight):
@@ -402,6 +526,8 @@
     tiles = ecount * cap // 8
     rows = ecount * cap
     vmem, any_space = pl.BlockSpec(memory_space=pltpu.VMEM), pl.BlockSpec(memory_space=pl.ANY)
+    hbm = pl.BlockSpec(memory_space=pltpu.HBM)
+    sources = ecount // SIDE
     dma = pltpu.SemaphoreType.DMA
     gate_out, linear_out, mix = pl.pallas_call(
         functools.partial(kernel, n_fs, n_tp),
@@ -410,21 +536,25 @@
             jax.ShapeDtypeStruct((ecount, stripe, hid), BF),
             jax.ShapeDtypeStruct((tok, fcols), BF),
         ),
-        in_specs=[vmem] * 3 + [any_space] * 4,
+        in_specs=[hbm] * 7,
         out_specs=(any_space, any_space, vmem),
         scratch_shapes=[
+            pltpu.VMEM((top, tok), jnp.int32),
+            pltpu.VMEM((top, tok), F32),
+            pltpu.VMEM((width // hid, hid), F32),
             pltpu.VMEM((ecount, stripe, hid), F32),
             pltpu.VMEM((ecount, stripe, hid), F32),
             pltpu.VMEM((tok, fcols), BF),
-            pltpu.VMEM((n_tp, fcols, hid), BF),
+            pltpu.VMEM((SIDE, width // SIDE, hid), BF),
             pltpu.VMEM((ecount, stripe, 2 * hid), BF),
             pltpu.VMEM((ecount, stripe, 2 * hid), BF),
             pltpu.VMEM((tiles, 8, fcols), BF),
             pltpu.VMEM((n_tp, tiles, 8, fcols), BF),
-            pltpu.VMEM((n_tp, tiles, 8, hid), BF),
-            pltpu.VMEM((n_tp, fcols, hid), BF),
-            pltpu.VMEM((tiles, 8, fcols), BF),
-            pltpu.VMEM((tiles, 8, fcols), BF),
+            pltpu.VMEM((sources // 2, SIDE, cap // 4, 8, hid), BF),
+            pltpu.VMEM((SIDE, SIDE, sources // 2, cap // 4, 8, hid), BF),
+            pltpu.VMEM((SIDE, SIDE, width // SIDE, hid), BF),
+            pltpu.VMEM((SIDE, sources, cap // 8, 8, fcols), BF),
+            pltpu.VMEM((ecount, cap // 8, 8, fcols), BF),
             pltpu.VMEM((ecount, tok), F32),
             pltpu.VMEM((ecount, tok), F32),
             pltpu.VMEM((rows, tok), F32),
@@ -432,23 +562,27 @@
             pltpu.VMEM((tok, rows), BF),
             pltpu.VMEM((tok, rows), BF),
             pltpu.VMEM((rows, 2 * hid), F32),
-            pltpu.VMEM((rows, fcols), F32),
-            dma((6,)),
+            pltpu.VMEM((rows // SIDE, width // SIDE), F32),
+            dma((9,)),
             dma((n_fs,)),
             dma((n_fs,)),
             dma((n_fs,)),
             dma((n_fs,)),
             dma((n_fs,)),
             dma((n_fs,)),
-            dma((n_tp,)),
-            dma((n_tp,)),
+            dma((SIDE,)),
+            dma((SIDE,)),
+            dma((16,)),
+            dma((16,)),
             dma((40,)),
             dma((40,)),
-            dma((40,)),
-            dma((40,)),
+            dma((SIDE,)),
+            dma((SIDE,)),
+            dma((16,)),
+            dma((16,)),
         ],
         compiler_params=pltpu.CompilerParams(
-            collective_id=0, has_side_effects=True, vmem_limit_bytes=48 * 1024 * 1024
+            collective_id=0, has_side_effects=True, vmem_limit_bytes=67043328
         ),
     )(
         experts.T,
@@ -457,7 +591,7 @@
         tokens,
         gate_master,
         linear_master,
-        down_weight.reshape(n_tp, fcols, hid),
+        down_weight.reshape(SIDE, width // SIDE, hid),
     )
     shape = (1, width, hid)
     return gate_out.reshape(shape), linear_out.reshape(shape), mix

time: 121 us -> 107 us (0.88)
  Pallas kernels: 112 us -> 103 us
  local copies, waits for them, and re-layouts: 8.11 us -> 3.34 us
    pallas_call x1, Pallas kernels: 112 us -> 103 us  [on_device(): pl.pallas_call(functools.partial(kernel, n_fs, n_tp), out_shape=(jax.Shap...]
    unnamed x17 -> x7, local copies, waits for them, and re-layouts: 8.11 us -> 3.34 us
where the time goes in v3:
time: 107 us
  Pallas kernels  103 us (96%)
  local copies, waits for them, and re-layouts  3.34 us (3%)
    pallas_call x1, Pallas kernels, on_device(): pl.pallas_call(functools.partial(kernel, n_fs, n_tp), out_shape=(jax.Shap...  103 us
    unnamed x7, local copies, waits for them, and re-layouts  3.34 us

profile of v3, /device:TPU:1, one launch (start us, length us, event | category | flops | bytes accessed | tf_op | source)
XLA Modules:
  0.0 107.0 jit_solution(319805699501965410)
XLA Ops:
  0.6 103.0 %shard_map.94 = (bf16[32,64,128]{2,1,0:T(8,128)(2,1)}, bf16[32,64,128]{2,1,0:T(8,128)(2,1)}, bf16[128,128]{1,0:T(8,128)(2,1)}) custom-call(s32[4,128]{1,0:T(4,128)} %bitcast.10, f32[4,128]{1,0:T(4,128)} %bitcast.11, f32[16,128]{1,0:T(8,128)} %bitcast.9, bf16[128,2048]{1,0:T(8,128)(2,1)} %tokens_hbm.1, f32[32,64,128]{2,1,0:T(8,128)} %gate_hbm.1, ...), custom_call_target="tpu_custom_call" | custom-call | tf_op jit(solution)/shard_map/pallas_call | solution.py:532
  103.6 0.0 copy-start
  103.6 1.9 %copy.13 = bf16[1,2048,128]{2,1,0:T(8,128)(2,1)} copy(bf16[1,2048,128]{2,1,0:T(8,128)(2,1)} %bitcast.7) | data formatting | bytes 1048576
  105.5 0.0 copy-done
  105.5 0.0 copy-start.1
  105.5 0.8 copy.14
  106.3 0.0 copy-done.1
  106.3 0.6 copy.15
Async XLA Ops:
  103.6 1.9 %copy-start = (bf16[32,64,128]{2,1,0:T(8,128)(2,1)S(1)}, bf16[32,64,128]{2,1,0:T(8,128)(2,1)}, u32[]{:S(2)}) copy-start(bf16[32,64,128]{2,1,0:T(8,128)(2,1)} %get-tuple-element.7) | copy-start | bytes 1572868
  105.5 0.8 copy-start.1

commit v4 on v3

--- a/solution.py
+++ b/solution.py
@@ -374,27 +374,30 @@
         dx.second(k)
     tg.rest()
 
-    ratio = (2 * stripe) // fcols
-
-    def multiply(chip):
-        for j in range(ratio):
-            block = chip * ratio + j
-            lhs = t_grid[block].reshape(rows, fcols)
-            if ratio == 1:
-                rhs = w_recv[pl.ds(chip * 2, 2)].reshape(fcols, 2 * hid)
-            else:
-                rhs = w_recv[chip * 2 + j // (ratio // 2), (j % (ratio // 2)) * fcols :][:fcols]
-            acc[...] += jnp.dot(lhs, rhs, preferred_element_type=F32)
-
-    weights_copy(0, 1, peer(0, 1), source(0, 1)).wait_recv()
-    multiply(z)
-
-    @pl.loop(0, n_z - 1)
-    def _(k):
-        dz = turn(k)
+    def lhs(chip):
+        return t_grid[chip].reshape(rows, fcols)
+
+    def rhs(chip):
+        return w_recv[pl.ds(chip * 2, 2)].reshape(fcols, 2 * hid)
+
+    def multiply(one, other):
+        acc[...] += jnp.dot(
+            jnp.concatenate([lhs(one), lhs(other)], axis=1),
+            jnp.concatenate([rhs(one), rhs(other)], axis=0),
+            preferred_element_type=F32,
+        )
+
+    def weights_of(dz):
         for dc in (0, 1):
             weights_copy(dz, dc, peer(dz, dc), source(dz, dc)).wait_recv()
-        multiply((z - dz + n_z) % n_z)
+        return (z - dz + n_z) % n_z
+
+    weights_copy(0, 1, peer(0, 1), source(0, 1)).wait_recv()
+    multiply(z, weights_of(n_z // 2))
+
+    @pl.loop(1, n_z // 2)
+    def _(k):
+        multiply(weights_of(n_z // 2 - k), weights_of(n_z // 2 + k))
 
     stores = [
         pltpu.make_async_copy(w_recv.at[:, :, pl.ds(0, hid)], gate_out, local_sems.at[7]),
@@ -403,94 +406,135 @@
     for store in stores:
         store.start()
 
-    clamped = jnp.minimum(acc[:, 0:hid], clamp_limit)
-    linear = jnp.clip(acc[:, hid : 2 * hid], -clamp_limit, clamp_limit)
-    active = clamped * jax.nn.sigmoid(gate_slope * clamped) * (linear + 1.0)
-    a_send[...] = active.astype(BF).reshape(a_send.shape)
-
-    def active_x(k, slot):
+    n_q = a_send.shape[0]
+    offsets = (4, 5, 3, 0, 6, 2, 7, 1)
+    chunk = n_q // 2
+    span = rows // n_q
+    groups = (1, 3, 2)
+
+    def q_of(j):
+        return (z // 2 + offsets[j]) % n_q
+
+    def active_x(r, k, slot):
         to = (x + k) % SIDE
+        i = r * SIDE + k
         return remote(
-            a_send.at[:, to], a_grid.at[y, slot], ax_ssem.at[k], ax_rsem.at[k], {"tp": y * SIDE + to}
-        )
-
-    def active_ref(p, k, part):
+            a_send.at[pl.ds(r * chunk, chunk), to],
+            a_grid.at[y, slot, pl.ds(r * chunk, chunk)],
+            ax_ssem.at[i],
+            ax_rsem.at[i],
+            {"tp": y * SIDE + to},
+        )
+
+    def active_ref(p, item, part):
+        r, k = item // SIDE, item % SIDE
         block = a_grid.at[p, (x - k + SIDE) % SIDE]
-        half = a_grid.shape[2] // 2
-        return block if part is None else block.at[pl.ds(part * half, half)]
+        half = chunk // 2
+        if part is None:
+            return block.at[pl.ds(r * chunk, chunk)]
+        return block.at[pl.ds(r * chunk + part * half, half)]
 
     ay = Ring(active_ref, lambda p: {"tp": p * SIDE + x}, ay_ssem, ay_rsem, y)
-    groups = (1, 3, 2)
-    for k in groups:
-        active_x(k, x).start()
-    a_grid[y, x] = a_send[:, x]
-    ay.first(0)
+
+    for r in (0, 1):
+        for j in range(r * chunk, (r + 1) * chunk):
+            at = pl.ds(pl.multiple_of(q_of(j) * span, 8), span)
+            clamped = jnp.minimum(acc[at, 0:hid], clamp_limit)
+            linear = jnp.clip(acc[at, hid : 2 * hid], -clamp_limit, clamp_limit)
+            active = clamped * jax.nn.sigmoid(gate_slope * clamped) * (linear + 1.0)
+            a_send[j] = active.astype(BF).reshape(a_send.shape[1:])
+        for k in groups:
+            active_x(r, k, x).start()
+        at = pl.ds(r * chunk, chunk)
+        a_grid[y, x, at] = a_send[at, x]
+        if r == 0:
+            ay.first(0)
+
     acc2[...] = jnp.zeros_like(acc2)
-    share = acc2.shape[0]
-
-    def multiply_down(step, k):
-        p, g = (y + step + SIDE) % SIDE, (x - k + SIDE) % SIDE
-        acc2[...] += lax.dot_general(
-            a_grid[p, g].reshape(share, hid),
-            d_grid[p, g],
+    share = acc2.shape[1]
+
+    def multiply_down(r, step, k, k2):
+        p = (y + step + SIDE) % SIDE
+        g, g2 = (x - k + SIDE) % SIDE, (x - k2 + SIDE) % SIDE
+        at = pl.ds(r * chunk, chunk)
+        acc2[r] += lax.dot_general(
+            jnp.concatenate(
+                [a_grid[p, g, at].reshape(share, hid), a_grid[p, g2, at].reshape(share, hid)], axis=1
+            ),
+            jnp.concatenate([d_grid[p, g], d_grid[p, g2]], axis=1),
             (((1,), (1,)), ((), ())),
             preferred_element_type=F32,
         )
 
-    for k in (0,) + groups:
-        dx.last(k)
-    multiply_down(0, 0)
-    for k in groups:
-        active_x(k, (x - k + SIDE) % SIDE).wait_recv()
-        ay.first(k)
-    for k in groups:
-        multiply_down(0, k)
-    for k in (0,) + groups:
-        ay.second(k)
-        multiply_down(-1, k)
-        multiply_down(1, k)
-    for k in (0,) + groups:
-        ay.last(k)
-        multiply_down(2, k)
-
-    for p in range(SIDE):
-        part = acc2[:, p * fcols : (p + 1) * fcols].astype(BF)
-        r_send[p] = part.reshape(r_send.shape[1:])
-
-    def return_copy(q, core, p):
-        chip = q * SIDE + x
-        to = chip * 2 + core
+    def return_copy(j, p):
+        to = q_of(j) * SIDE + x
         return remote(
-            r_send.at[p, q * 2 + core],
+            r_send.at[p, j],
             r_recv.at[f],
-            r_ssem.at[(q * 2 + core) * SIDE + p],
+            r_ssem.at[j * SIDE + p],
             r_rsem.at[f],
             {"fs": to, "tp": y * SIDE + p},
         ), jnp.logical_and(to == f, p == x)
 
-    def each_return(act):
-        @pl.loop(0, n_z // SIDE)
-        def _(k):
-            q = (z // SIDE + n_z // SIDE // 2 + k) % (n_z // SIDE)
-            for core in (0, 1):
-                for p in range(SIDE):
-                    c, local = return_copy(q, core, p)
+    def each_return(r, act):
+        for j in range(r * chunk, (r + 1) * chunk):
+            for p in range(SIDE):
+                c, local = return_copy(j, p)
+                if offsets[j] != 0:
+                    act(c)
+                else:
 
                     @pl.when(jnp.logical_not(local))
                     def _():
                         act(c)
 
-    each_return(lambda c: c.start())
-
-    @pl.when(z % SIDE == x)
+    def give_back(r):
+        for p in range(SIDE):
+            part = acc2[r, :, p * fcols : (p + 1) * fcols].astype(BF)
+            r_send[p, pl.ds(r * chunk, chunk)] = part.reshape(chunk, *r_send.shape[2:])
+        each_return(r, lambda c: c.start())
+
+    for k in groups:
+        active_x(0, k, (x - k + SIDE) % SIDE).wait_recv()
+        ay.first(k)
+    for k in (0,) + groups:
+        dx.last(k)
+    multiply_down(0, 0, 0, 1)
+    multiply_down(0, 0, 3, 2)
+    for k in (0,) + groups:
+        ay.second(k)
+        if k > 0:
+            active_x(1, k, (x - k + SIDE) % SIDE).wait_recv()
+        ay.first(SIDE + k)
+    for step in (-1, 1):
+        multiply_down(0, step, 0, 1)
+        multiply_down(0, step, 3, 2)
+    for k in (0,) + groups:
+        ay.second(SIDE + k)
+    for k in (0,) + groups:
+        ay.last(k)
+    multiply_down(0, 2, 0, 1)
+    multiply_down(0, 2, 3, 2)
+    give_back(0)
+    for step in (0, -1, 1):
+        multiply_down(1, step, 0, 1)
+        multiply_down(1, step, 3, 2)
+    for k in (0,) + groups:
+        ay.last(SIDE + k)
+    multiply_down(1, 2, 0, 1)
+    multiply_down(1, 2, 3, 2)
+    give_back(1)
+
+    @pl.when(f % SIDE == x)
     def _():
-        r_recv[f] = r_send[x, (z // SIDE) * 2 + c]
+        r_recv[f] = r_send[x, offsets.index(0)]
 
     drain_all(tokens_copy)
     drain_all(weights_copy)
     for k in groups:
         down_y(k, y).wait_send()
-        active_x(k, x).wait_send()
+        active_x(0, k, x).wait_send()
+        active_x(1, k, x).wait_send()
     dx.drain()
     tg.drain()
     ay.drain()
@@ -499,14 +543,14 @@
 
     @pl.loop(0, n_fs)
     def _(e):
-        @pl.when(jnp.logical_not(jnp.logical_and(e == f, z % SIDE == x)))
+        @pl.when(jnp.logical_not(jnp.logical_and(e == f, f % SIDE == x)))
         def _():
             remote(
                 r_send.at[0, 0],
                 r_recv.at[e],
                 r_ssem.at[0],
                 r_rsem.at[e],
-                {"fs": e, "tp": y * SIDE + z % SIDE},
+                {"fs": e, "tp": y * SIDE + f % SIDE},
             ).wait_recv()
 
     back = r_recv[...].reshape(rows, fcols)
@@ -514,7 +558,19 @@
         low_v[...], back, preferred_element_type=F32
     )
     mix_out[...] = mix.astype(BF)
-    each_return(lambda c: c.wait_send())
+    each_return(0, lambda c: c.wait_send())
+    each_return(1, lambda c: c.wait_send())
+
+
+def copy_out(a, b, c, a_out, b_out, c_out, sems):
+    copies = [
+        pltpu.make_async_copy(src, dst, sems.at[i])
+        for i, (src, dst) in enumerate(((a, a_out), (b, b_out), (c, c_out)))
+    ]
+    for copy in copies:
+        copy.start()
+    for copy in copies:
+        copy.wait()
 
 
 def on_device(n_fs, n_tp, tokens, experts, routing, gain, gate_master, linear_master, down_weight):
@@ -550,8 +606,8 @@
             pltpu.VMEM((ecount, stripe, 2 * hid), BF),
             pltpu.VMEM((tiles, 8, fcols), BF),
             pltpu.VMEM((n_tp, tiles, 8, fcols), BF),
-            pltpu.VMEM((sources // 2, SIDE, cap // 4, 8, hid), BF),
-            pltpu.VMEM((SIDE, SIDE, sources // 2, cap // 4, 8, hid), BF),
+            pltpu.VMEM((sources, SIDE, cap // 8, 8, hid), BF),
+            pltpu.VMEM((SIDE, SIDE, sources, cap // 8, 8, hid), BF),
             pltpu.VMEM((SIDE, SIDE, width // SIDE, hid), BF),
             pltpu.VMEM((SIDE, sources, cap // 8, 8, fcols), BF),
             pltpu.VMEM((ecount, cap // 8, 8, fcols), BF),
@@ -562,7 +618,7 @@
             pltpu.VMEM((tok, rows), BF),
             pltpu.VMEM((tok, rows), BF),
             pltpu.VMEM((rows, 2 * hid), F32),
-            pltpu.VMEM((rows // SIDE, width // SIDE), F32),
+            pltpu.VMEM((2, rows // SIDE // 2, width // SIDE), F32),
             dma((9,)),
             dma((n_fs,)),
             dma((n_fs,)),
@@ -576,25 +632,37 @@
             dma((16,)),
             dma((40,)),
             dma((40,)),
-            dma((SIDE,)),
-            dma((SIDE,)),
-            dma((16,)),
-            dma((16,)),
+            dma((2 * SIDE,)),
+            dma((2 * SIDE,)),
+            dma((32,)),
+            dma((32,)),
         ],
         compiler_params=pltpu.CompilerParams(
-            collective_id=0, has_side_effects=True, vmem_limit_bytes=67043328
+            collective_id=0, has_side_effects=True, vmem_limit_bytes=48 * 1024 * 1024
         ),
     )(
-        experts.T,
-        routing.T,
-        gain.reshape(width // hid, hid),
-        tokens,
-        gate_master,
-        linear_master,
-        down_weight.reshape(SIDE, width // SIDE, hid),
+        *[
+            pltpu.with_memory_space_constraint(v, pltpu.HBM)
+            for v in (
+                experts.T,
+                routing.T,
+                gain.reshape(width // hid, hid),
+                tokens,
+                gate_master,
+                linear_master,
+                down_weight.reshape(SIDE, width // SIDE, hid),
+            )
+        ]
     )
     shape = (1, width, hid)
-    return gate_out.reshape(shape), linear_out.reshape(shape), mix
+    results = (gate_out.reshape(shape), linear_out.reshape(shape), mix)
+    return pl.pallas_call(
+        copy_out,
+        out_shape=tuple(jax.ShapeDtypeStruct(v.shape, v.dtype) for v in results),
+        in_specs=[vmem] * 3,
+        out_specs=(hbm,) * 3,
+        scratch_shapes=[dma((3,))],
+    )(*[pltpu.with_memory_space_constraint(v, pltpu.VMEM) for v in results])
 
 
 def solution(mesh):

time: 107 us -> 101 us (0.944)
  local copies, waits for them, and re-layouts: 3.34 us -> 0 us
  Pallas kernels: 103 us -> 101 us
    pallas_call x1, Pallas kernels: 103 us -> 99.6 us  [on_device(): pl.pallas_call(functools.partial(kernel, n_fs, n_tp), out_shape=(jax.Shap...]
    unnamed x7 -> x0, local copies, waits for them, and re-layouts: 3.34 us -> none
where the time goes in v4:
time: 101 us
  Pallas kernels  101 us (100%)
    pallas_call x1, Pallas kernels, on_device(): pl.pallas_call(functools.partial(kernel, n_fs, n_tp), out_shape=(jax.Shap...  99.6 us

profile of v4, /device:TPU:1, one launch (start us, length us, event | category | flops | bytes accessed | tf_op | source)
XLA Modules:
  0.0 101.2 jit_solution(5273007450551582743)
XLA Ops:
  0.6 99.6 %shard_map.94 = (bf16[32,64,128]{2,1,0:T(8,128)(2,1)S(1)}, bf16[32,64,128]{2,1,0:T(8,128)(2,1)S(1)}, bf16[128,128]{1,0:T(8,128)(2,1)S(1)}) custom-call(s32[4,128]{1,0:T(4,128)} %bitcast.10, f32[4,128]{1,0:T(4,128)} %bitcast.11, f32[16,128]{1,0:T(8,128)} %bitcast.9, bf16[128,2048]{1,0:T(8,128)(2,1)} %tokens_hbm.1, f32[32,64,128]{2,1,0:T(8,128)} %gate_hbm.1, ...), custom_call_target="tpu_custom_call" | custom-call | tf_op jit(solution)/shard_map/pallas_call | solution.py:588
  100.2 1.0 shard_map.95

commit v5 on v4

--- a/solution.py
+++ b/solution.py
@@ -12,6 +12,7 @@
 BF = jnp.bfloat16
 F32 = jnp.float32
 MESH = pl.DeviceIdType.MESH
+CHUNKS = 4
 SIDE = 4
 
 
@@ -173,7 +174,6 @@
     high_v,
     low_v,
     acc,
-    acc2,
     local_sems,
     t_ssem,
     t_rsem,
@@ -187,10 +187,8 @@
     dx_rsem,
     tg_ssem,
     tg_rsem,
-    ax_ssem,
-    ax_rsem,
-    ay_ssem,
-    ay_rsem,
+    a_ssem,
+    a_rsem,
 ):
     f, t = lax.axis_index("fs"), lax.axis_index("tp")
     n_z = n_fs // 2
@@ -408,63 +406,58 @@
 
     n_q = a_send.shape[0]
     offsets = (4, 5, 3, 0, 6, 2, 7, 1)
-    chunk = n_q // 2
+    chunk = n_q // CHUNKS
     span = rows // n_q
     groups = (1, 3, 2)
+    others = sorted(
+        ((a, b) for a in range(SIDE) for b in range(SIDE) if (a, b) != (0, 0)),
+        key=lambda ab: -min(ab[0], SIDE - ab[0]) - min(ab[1], SIDE - ab[1]),
+    )
 
     def q_of(j):
         return (z // 2 + offsets[j]) % n_q
 
-    def active_x(r, k, slot):
-        to = (x + k) % SIDE
-        i = r * SIDE + k
+    def active_copy(r, dy_, dx_, to, at):
+        i = (r * SIDE + dy_) * SIDE + dx_
         return remote(
-            a_send.at[pl.ds(r * chunk, chunk), to],
-            a_grid.at[y, slot, pl.ds(r * chunk, chunk)],
-            ax_ssem.at[i],
-            ax_rsem.at[i],
-            {"tp": y * SIDE + to},
+            a_send.at[pl.ds(r * chunk, chunk), to[1]],
+            a_grid.at[at[0], at[1], pl.ds(r * chunk, chunk)],
+            a_ssem.at[i],
+            a_rsem.at[i],
+            {"tp": to[0] * SIDE + to[1]},
         )
 
-    def active_ref(p, item, part):
-        r, k = item // SIDE, item % SIDE
-        block = a_grid.at[p, (x - k + SIDE) % SIDE]
-        half = chunk // 2
-        if part is None:
-            return block.at[pl.ds(r * chunk, chunk)]
-        return block.at[pl.ds(r * chunk + part * half, half)]
-
-    ay = Ring(active_ref, lambda p: {"tp": p * SIDE + x}, ay_ssem, ay_rsem, y)
-
-    for r in (0, 1):
+    def ahead(dy_, dx_):
+        return (y + dy_) % SIDE, (x + dx_) % SIDE
+
+    def behind(dy_, dx_):
+        return (y - dy_ + SIDE) % SIDE, (x - dx_ + SIDE) % SIDE
+
+    for r in range(CHUNKS):
         for j in range(r * chunk, (r + 1) * chunk):
             at = pl.ds(pl.multiple_of(q_of(j) * span, 8), span)
             clamped = jnp.minimum(acc[at, 0:hid], clamp_limit)
             linear = jnp.clip(acc[at, hid : 2 * hid], -clamp_limit, clamp_limit)
             active = clamped * jax.nn.sigmoid(gate_slope * clamped) * (linear + 1.0)
             a_send[j] = active.astype(BF).reshape(a_send.shape[1:])
-        for k in groups:
-            active_x(r, k, x).start()
+        for dy_, dx_ in others:
+            active_copy(r, dy_, dx_, ahead(dy_, dx_), (y, x)).start()
+    a_grid[y, x] = a_send[:, x]
+    share = chunk * span // SIDE
+    for k in (0,) + groups:
+        dx.last(k)
+
+    def multiply_down(r):
         at = pl.ds(r * chunk, chunk)
-        a_grid[y, x, at] = a_send[at, x]
-        if r == 0:
-            ay.first(0)
-
-    acc2[...] = jnp.zeros_like(acc2)
-    share = acc2.shape[1]
-
-    def multiply_down(r, step, k, k2):
-        p = (y + step + SIDE) % SIDE
-        g, g2 = (x - k + SIDE) % SIDE, (x - k2 + SIDE) % SIDE
-        at = pl.ds(r * chunk, chunk)
-        acc2[r] += lax.dot_general(
-            jnp.concatenate(
-                [a_grid[p, g, at].reshape(share, hid), a_grid[p, g2, at].reshape(share, hid)], axis=1
-            ),
-            jnp.concatenate([d_grid[p, g], d_grid[p, g2]], axis=1),
-            (((1,), (1,)), ((), ())),
-            preferred_element_type=F32,
-        )
+        total = jnp.zeros((share, d_grid.shape[2]), F32)
+        for p in range(SIDE):
+            total = total + lax.dot_general(
+                jnp.concatenate([a_grid[p, g, at].reshape(share, hid) for g in range(SIDE)], axis=1),
+                jnp.concatenate([d_grid[p, g] for g in range(SIDE)], axis=1),
+                (((1,), (1,)), ((), ())),
+                preferred_element_type=F32,
+            )
+        return total
 
     def return_copy(j, p):
         to = q_of(j) * SIDE + x
@@ -488,42 +481,14 @@
                     def _():
                         act(c)
 
-    def give_back(r):
+    for r in range(CHUNKS):
+        for dy_, dx_ in others:
+            active_copy(r, dy_, dx_, ahead(dy_, dx_), behind(dy_, dx_)).wait_recv()
+        total = multiply_down(r)
         for p in range(SIDE):
-            part = acc2[r, :, p * fcols : (p + 1) * fcols].astype(BF)
+            part = total[:, p * fcols : (p + 1) * fcols].astype(BF)
             r_send[p, pl.ds(r * chunk, chunk)] = part.reshape(chunk, *r_send.shape[2:])
         each_return(r, lambda c: c.start())
-
-    for k in groups:
-        active_x(0, k, (x - k + SIDE) % SIDE).wait_recv()
-        ay.first(k)
-    for k in (0,) + groups:
-        dx.last(k)
-    multiply_down(0, 0, 0, 1)
-    multiply_down(0, 0, 3, 2)
-    for k in (0,) + groups:
-        ay.second(k)
-        if k > 0:
-            active_x(1, k, (x - k + SIDE) % SIDE).wait_recv()
-        ay.first(SIDE + k)
-    for step in (-1, 1):
-        multiply_down(0, step, 0, 1)
-        multiply_down(0, step, 3, 2)
-    for k in (0,) + groups:
-        ay.second(SIDE + k)
-    for k in (0,) + groups:
-        ay.last(k)
-    multiply_down(0, 2, 0, 1)
-    multiply_down(0, 2, 3, 2)
-    give_back(0)
-    for step in (0, -1, 1):
-        multiply_down(1, step, 0, 1)
-        multiply_down(1, step, 3, 2)
-    for k in (0,) + groups:
-        ay.last(SIDE + k)
-    multiply_down(1, 2, 0, 1)
-    multiply_down(1, 2, 3, 2)
-    give_back(1)
 
     @pl.when(f % SIDE == x)
     def _():
@@ -533,11 +498,11 @@
     drain_all(weights_copy)
     for k in groups:
         down_y(k, y).wait_send()
-        active_x(0, k, x).wait_send()
-        active_x(1, k, x).wait_send()
     dx.drain()
     tg.drain()
-    ay.drain()
+    for r in range(CHUNKS):
+        for dy_, dx_ in others:
+            active_copy(r, dy_, dx_, ahead(dy_, dx_), (y, x)).wait_send()
     for store in stores:
         store.wait()
 
@@ -558,8 +523,8 @@
         low_v[...], back, preferred_element_type=F32
     )
     mix_out[...] = mix.astype(BF)
-    each_return(0, lambda c: c.wait_send())
-    each_return(1, lambda c: c.wait_send())
+    for r in range(CHUNKS):
+        each_return(r, lambda c: c.wait_send())
 
 
 def copy_out(a, b, c, a_out, b_out, c_out, sems):
@@ -618,7 +583,6 @@
             pltpu.VMEM((tok, rows), BF),
             pltpu.VMEM((tok, rows), BF),
             pltpu.VMEM((rows, 2 * hid), F32),
-            pltpu.VMEM((2, rows // SIDE // 2, width // SIDE), F32),
             dma((9,)),
             dma((n_fs,)),
             dma((n_fs,)),
@@ -632,10 +596,8 @@
             dma((16,)),
             dma((40,)),
             dma((40,)),
-            dma((2 * SIDE,)),
-            dma((2 * SIDE,)),
-            dma((32,)),
-            dma((32,)),
+            dma((CHUNKS * n_tp,)),
+            dma((CHUNKS * n_tp,)),
         ],
         compiler_params=pltpu.CompilerParams(
             collective_id=0, has_side_effects=True, vmem_limit_bytes=48 * 1024 * 1024

time: 101 us -> 98.2 us (0.972)
  Pallas kernels: 101 us -> 97 us
    pallas_call x1, Pallas kernels: 99.6 us -> 96 us  [on_device(): pl.pallas_call(functools.partial(kernel, n_fs, n_tp), out_shape=(jax.Shap...]
where the time goes in v5:
time: 98.2 us; the launch traced here: 97.6 us
  Pallas kernels  97 us (99%)
    pallas_call x1, Pallas kernels, on_device(): pl.pallas_call(functools.partial(kernel, n_fs, n_tp), out_shape=(jax.Shap...  96 us

profile of v5, /device:TPU:1, one launch (start us, length us, event | category | flops | bytes accessed | tf_op | source)
XLA Modules:
  0.0 97.6 jit_solution(17383441253989692934)
XLA Ops:
  0.6 96.0 %shard_map.94 = (bf16[32,64,128]{2,1,0:T(8,128)(2,1)S(1)}, bf16[32,64,128]{2,1,0:T(8,128)(2,1)S(1)}, bf16[128,128]{1,0:T(8,128)(2,1)S(1)}) custom-call(s32[4,128]{1,0:T(4,128)} %bitcast.10, f32[4,128]{1,0:T(4,128)} %bitcast.11, f32[16,128]{1,0:T(8,128)} %bitcast.9, bf16[128,2048]{1,0:T(8,128)(2,1)} %tokens_hbm.1, f32[32,64,128]{2,1,0:T(8,128)} %gate_hbm.1, ...), custom_call_target="tpu_custom_call" | custom-call | tf_op jit(solution)/shard_map/pallas_call | solution.py:553
  96.6 1.0 %shard_map.95 = (bf16[1,2048,128]{2,1,0:T(8,128)(2,1)}, bf16[1,2048,128]{2,1,0:T(8,128)(2,1)}, bf16[128,128]{1,0:T(8,128)(2,1)}) custom-call(bf16[1,2048,128]{2,1,0:T(8,128)(2,1)S(1)} %bitcast.6, bf16[1,2048,128]{2,1,0:T(8,128)(2,1)S(1)} %bitcast.7, bf16[128,128]{1,0:T(8,128)(2,1)S(1)} %get-tuple-element.8.c), custom_call_target="tpu_custom_call" | custom-call | tf_op jit(solution)/shard_map/pallas_call | solution.py:621

commit v6 on v5

--- a/solution.py
+++ b/solution.py
@@ -33,7 +33,6 @@
         self.y, self.x = t // SIDE, t % SIDE
         tiles = grid.shape[1]
         self.half, self.quarter = tiles // 2, tiles // 4
-        self.sent = []
 
     def at(self, h, a, b):
         dx, dy = (a, b) if h == 0 else (b, a)
@@ -43,13 +42,11 @@
         start = h * self.half + (self.quarter if part == 1 else 0)
         size = self.half if part is None else self.quarter
         ref = self.grid.at[self.at(h, a, b), pl.ds(start, size)]
-        k = h * 20 + slot
-        return remote(ref, ref, self.send_sems.at[k], self.recv_sems.at[k], {"tp": self.at(h, *to)})
+        k = 0 if slot > 5 and slot % 4 > 1 else 1 + h * 12 + (slot if slot < 4 else 4 + slot // 4 * 2 - 2 + slot % 4)
+        return remote(ref, ref, self.send_sems.at[0], self.recv_sems.at[k], {"tp": self.at(h, *to)})
 
     def send(self, h, slot, a, b, part, to):
-        c = self.copy(h, slot, a, b, part, to)
-        c.start()
-        self.sent.append(c)
+        self.copy(h, slot, a, b, part, to).start()
 
     def recv(self, h, slot, a, b, part):
         self.copy(h, slot, a, b, part, (1, 0)).wait_recv()
@@ -89,35 +86,33 @@
             self.turn(h, 2, 1)
         for h in (0, 1):
             self.turn(h, 3, 2)
-        for h in (0, 1):
-            for i, a in enumerate((0, -1, 1, 2)):
-                self.recv(h, 6 + 4 * i, a, 2, 0)
-                self.recv(h, 7 + 4 * i, a, 2, 1)
+        self.whole(SIDE).wait_recv()
+
+    def whole(self, blocks):
+        ref = self.grid.at[pl.ds(0, blocks)]
+        return remote(ref, ref, self.send_sems.at[0], self.recv_sems.at[0], {"tp": self.at(0, 1, 0)})
 
     def drain(self):
-        for c in self.sent:
-            c.wait_send()
+        self.whole(SIDE * SIDE - 1).wait_send()
 
 
 class Ring:
     def __init__(self, ref_of, device_of, send_sems, recv_sems, pos):
         self.ref_of, self.device_of, self.pos = ref_of, device_of, pos
-        self.send_sems, self.recv_sems, self.sent = send_sems, recv_sems, []
+        self.send_sems, self.recv_sems = send_sems, recv_sems
 
     def at(self, step):
         return (self.pos + step + SIDE) % SIDE
 
     def copy(self, item, slot, step, part, to):
         ref = self.ref_of(self.at(step), item, part)
-        k = item * 4 + slot
+        k = 0 if slot > 1 else 1 + item * 2 + slot
         return remote(
-            ref, ref, self.send_sems.at[k], self.recv_sems.at[k], self.device_of(self.at(to))
+            ref, ref, self.send_sems.at[0], self.recv_sems.at[k], self.device_of(self.at(to))
         )
 
     def send(self, item, slot, step, part, to):
-        c = self.copy(item, slot, step, part, to)
-        c.start()
-        self.sent.append(c)
+        self.copy(item, slot, step, part, to).start()
 
     def first(self, item):
         self.send(item, 0, 0, None, 1)
@@ -129,13 +124,10 @@
         self.copy(item, 1, 1, None, 1).wait_recv()
         self.send(item, 3, 1, 1, -1)
 
-    def last(self, item):
-        self.copy(item, 2, 2, 0, 1).wait_recv()
-        self.copy(item, 3, 2, 1, 1).wait_recv()
-
-    def drain(self):
-        for c in self.sent:
-            c.wait_send()
+    def whole(self, ref):
+        return remote(
+            ref, ref, self.send_sems.at[0], self.recv_sems.at[0], self.device_of(self.at(1))
+        )
 
 
 def kernel(
@@ -165,6 +157,7 @@
     a_send,
     a_grid,
     d_grid,
+    d_turned,
     r_send,
     r_recv,
     slot_v,
@@ -255,7 +248,6 @@
         hit = slot_v[pl.ds(e, 1), :] == places
         at = pl.ds(pl.multiple_of(e * cap, 8), cap)
         pick_v[at, :] = jnp.where(hit, 1.0, 0.0)
-        mixer_v[at, :] = jnp.where(hit, weight_v[pl.ds(e, 1), :], 0.0)
 
     loads[0].wait()
     sent = jnp.dot(pick_v[...].astype(BF), tok_v[...], preferred_element_type=F32)
@@ -283,57 +275,39 @@
     def peer(dz, dc):
         return ((z + dz) % n_z) * 2 + (c + dc) % 2
 
-    def source(dz, dc):
-        return ((z - dz + n_z) % n_z) * 2 + (c + dc) % 2
-
     def turn(k):
         return (n_z // 2 + (1 - 2 * (k % 2)) * ((k + 1) // 2)) % n_z
 
-    def tokens_copy(dz, dc, to, slot):
-        i = dz * 2 + dc
+    def tokens_copy(k, to, slot, count=1):
         return remote(
-            t_send.at[tile_span(to)],
-            t_grid.at[t, tile_span(slot)],
-            t_ssem.at[i],
-            t_rsem.at[i],
-            {"fs": to},
-        )
-
-    def weights_copy(dz, dc, to, slot):
-        i = dz * 2 + dc
-        return remote(w_send.at[to], w_recv.at[slot], w_ssem.at[i], w_rsem.at[i], {"fs": to})
-
-    def start_all(copy):
+            t_send.at[pl.ds(to * per, count * per)],
+            t_grid.at[t, pl.ds(slot * per, count * per)],
+            t_ssem.at[0],
+            t_rsem.at[0],
+            {"fs": to if count == 1 else (f + 1) % n_fs},
+        )
+
+    def weights_copy(k, to, slot, count=1):
+        i = (k + 1) // 2
+        src, dst = w_send.at[pl.ds(to, count)], w_recv.at[pl.ds(slot, count)]
+        device = to if count == 1 else (f + 1) % n_fs
+        return remote(src, dst, w_ssem.at[0], w_rsem.at[i], {"fs": device})
+
+    def start_all(copy, core):
+        dc = (core + c) % 2
+
         @pl.loop(0, n_z - 1)
         def _(k):
-            dz = turn(k)
-            for dc in (0, 1):
-                copy(dz, dc, peer(dz, dc), f).start()
-
-        copy(0, 1, peer(0, 1), f).start()
-
-    def recv_all(copy):
-        copy(0, 1, peer(0, 1), source(0, 1)).wait_recv()
-
-        @pl.loop(0, n_z - 1)
-        def _(k):
-            dz = turn(k)
-            for dc in (0, 1):
-                copy(dz, dc, peer(dz, dc), source(dz, dc)).wait_recv()
-
-    def drain_all(copy):
-        copy(0, 1, peer(0, 1), f).wait_send()
-
-        @pl.loop(0, n_z - 1)
-        def _(k):
-            dz = turn(k)
-            for dc in (0, 1):
-                copy(dz, dc, peer(dz, dc), f).wait_send()
+            copy(k, peer(turn(k), dc), f).start()
+
+        @pl.when(dc == 1)
+        def _():
+            copy(n_z - 1, peer(0, 1), f).start()
 
     def down_y(k, slot):
         to = (y + k) % SIDE
         return remote(
-            down_v.at[to], d_grid.at[slot, x], dy_ssem.at[k], dy_rsem.at[k], {"tp": to * SIDE + x}
+            down_v.at[to], d_grid.at[slot, x], dy_ssem.at[0], dy_rsem.at[k], {"tp": to * SIDE + x}
         )
 
     def down_ref(p, k, part):
@@ -343,8 +317,10 @@
 
     dx = Ring(down_ref, lambda p: {"tp": y * SIDE + p}, dx_ssem, dx_rsem, x)
 
-    start_all(tokens_copy)
-    start_all(weights_copy)
+    start_all(tokens_copy, 0)
+    start_all(tokens_copy, 1)
+    start_all(weights_copy, 0)
+    start_all(weights_copy, 1)
 
     for k in (1, 3, 2):
         down_y(k, y).start()
@@ -353,6 +329,12 @@
 
     t_grid[t, tile_span(f)] = t_send[tile_span(f)]
     w_recv[f] = w_send[f]
+    @pl.loop(0, n_fs)
+    def _(e):
+        hit = slot_v[pl.ds(e, 1), :] == places
+        at = pl.ds(pl.multiple_of(e * cap, 8), cap)
+        mixer_v[at, :] = jnp.where(hit, weight_v[pl.ds(e, 1), :], 0.0)
+
     for j in range(rows // 128):
         at = slice(j * 128, (j + 1) * 128)
         turned = mixer_v[at, :].T
@@ -365,12 +347,19 @@
         down_y(k, (y - k + SIDE) % SIDE).wait_recv()
         dx.first(k)
 
-    recv_all(tokens_copy)
+    tokens_copy(0, 0, 0, n_fs - 1).wait_recv()
     tg = Torus(t_grid, tg_ssem, tg_rsem, t)
     tg.own()
     for k in (0, 1, 3, 2):
         dx.second(k)
     tg.rest()
+    dx.whole(d_grid.at[0]).wait_recv()
+
+    @pl.loop(0, SIDE)
+    def _(p):
+        for g in range(SIDE):
+            d_turned[p, g * hid : (g + 1) * hid, :] = d_grid[p, g].T
+
 
     def lhs(chip):
         return t_grid[chip].reshape(rows, fcols)
@@ -385,17 +374,14 @@
             preferred_element_type=F32,
         )
 
-    def weights_of(dz):
-        for dc in (0, 1):
-            weights_copy(dz, dc, peer(dz, dc), source(dz, dc)).wait_recv()
-        return (z - dz + n_z) % n_z
-
-    weights_copy(0, 1, peer(0, 1), source(0, 1)).wait_recv()
-    multiply(z, weights_of(n_z // 2))
+    weights_copy(n_z - 1, peer(0, 1), peer(0, 1)).wait_recv()
+    weights_copy(0, 0, 0, 2).wait_recv()
+    multiply(z, (z + n_z // 2) % n_z)
 
     @pl.loop(1, n_z // 2)
     def _(k):
-        multiply(weights_of(n_z // 2 - k), weights_of(n_z // 2 + k))
+        weights_copy(2 * k, 0, 0, 4).wait_recv()
+        multiply((z + n_z // 2 + k) % n_z, (z + n_z // 2 - k) % n_z)
 
     stores = [
         pltpu.make_async_copy(w_recv.at[:, :, pl.ds(0, hid)], gate_out, local_sems.at[7]),
@@ -405,7 +391,7 @@
         store.start()
 
     n_q = a_send.shape[0]
-    offsets = (4, 5, 3, 0, 6, 2, 7, 1)
+    offsets = (4, 5, 3, 6, 2, 1, 7, 0)
     chunk = n_q // CHUNKS
     span = rows // n_q
     groups = (1, 3, 2)
@@ -417,21 +403,21 @@
     def q_of(j):
         return (z // 2 + offsets[j]) % n_q
 
-    def active_copy(r, dy_, dx_, to, at):
-        i = (r * SIDE + dy_) * SIDE + dx_
+    def active_copy(r, to):
         return remote(
-            a_send.at[pl.ds(r * chunk, chunk), to[1]],
-            a_grid.at[at[0], at[1], pl.ds(r * chunk, chunk)],
-            a_ssem.at[i],
-            a_rsem.at[i],
-            {"tp": to[0] * SIDE + to[1]},
+            a_send.at[pl.ds(r * chunk, chunk), to % SIDE],
+            a_grid.at[t, pl.ds(r * chunk, chunk)],
+            a_ssem.at[0],
+            a_rsem.at[r],
+            {"tp": to},
         )
 
     def ahead(dy_, dx_):
-        return (y + dy_) % SIDE, (x + dx_) % SIDE
-
-    def behind(dy_, dx_):
-        return (y - dy_ + SIDE) % SIDE, (x - dx_ + SIDE) % SIDE
+        return (y + dy_) % SIDE * SIDE + (x + dx_) % SIDE
+
+    def arrived(at):
+        ref = a_grid.at[pl.ds(0, n_tp - 1), at]
+        return lambda r: remote(ref, ref, a_ssem.at[0], a_rsem.at[r], {"tp": ahead(0, 1)})
 
     for r in range(CHUNKS):
         for j in range(r * chunk, (r + 1) * chunk):
@@ -441,20 +427,20 @@
             active = clamped * jax.nn.sigmoid(gate_slope * clamped) * (linear + 1.0)
             a_send[j] = active.astype(BF).reshape(a_send.shape[1:])
         for dy_, dx_ in others:
-            active_copy(r, dy_, dx_, ahead(dy_, dx_), (y, x)).start()
-    a_grid[y, x] = a_send[:, x]
+            active_copy(r, ahead(dy_, dx_)).start()
+    a_grid[t] = a_send[:, x]
     share = chunk * span // SIDE
-    for k in (0,) + groups:
-        dx.last(k)
 
     def multiply_down(r):
         at = pl.ds(r * chunk, chunk)
-        total = jnp.zeros((share, d_grid.shape[2]), F32)
+        total = jnp.zeros((share, d_turned.shape[2]), F32)
         for p in range(SIDE):
             total = total + lax.dot_general(
-                jnp.concatenate([a_grid[p, g, at].reshape(share, hid) for g in range(SIDE)], axis=1),
-                jnp.concatenate([d_grid[p, g] for g in range(SIDE)], axis=1),
-                (((1,), (1,)), ((), ())),
+                jnp.concatenate(
+                    [a_grid[p * SIDE + g, at].reshape(share, hid) for g in range(SIDE)], axis=1
+                ),
+                d_turned[p],
+                (((1,), (0,)), ((), ())),
                 preferred_element_type=F32,
             )
         return total
@@ -464,8 +450,8 @@
         return remote(
             r_send.at[p, j],
             r_recv.at[f],
-            r_ssem.at[j * SIDE + p],
-            r_rsem.at[f],
+            r_ssem.at[0],
+            r_rsem.at[0],
             {"fs": to, "tp": y * SIDE + p},
         ), jnp.logical_and(to == f, p == x)
 
@@ -481,9 +467,9 @@
                     def _():
                         act(c)
 
+    weights_copy(0, 0, 0, n_fs - 1).wait_send()
     for r in range(CHUNKS):
-        for dy_, dx_ in others:
-            active_copy(r, dy_, dx_, ahead(dy_, dx_), behind(dy_, dx_)).wait_recv()
+        arrived(pl.ds(0, chunk))(r).wait_recv()
         total = multiply_down(r)
         for p in range(SIDE):
             part = total[:, p * fcols : (p + 1) * fcols].astype(BF)
@@ -494,37 +480,47 @@
     def _():
         r_recv[f] = r_send[x, offsets.index(0)]
 
-    drain_all(tokens_copy)
-    drain_all(weights_copy)
-    for k in groups:
-        down_y(k, y).wait_send()
-    dx.drain()
+    tokens_copy(0, 0, 0, n_fs - 1).wait_send()
+    remote(
+        down_v.at[pl.ds(1, SIDE - 1)],
+        d_grid.at[0, pl.ds(1, SIDE - 1)],
+        dy_ssem.at[0],
+        dy_rsem.at[1],
+        {"tp": ahead(1, 0)},
+    ).wait_send()
+    dx.whole(d_grid.at[pl.ds(0, SIDE - 1)]).wait_send()
     tg.drain()
-    for r in range(CHUNKS):
-        for dy_, dx_ in others:
-            active_copy(r, dy_, dx_, ahead(dy_, dx_), (y, x)).wait_send()
+    arrived(pl.ds(0, n_q))(0).wait_send()
     for store in stores:
         store.wait()
 
-    @pl.loop(0, n_fs)
-    def _(e):
-        @pl.when(jnp.logical_not(jnp.logical_and(e == f, f % SIDE == x)))
-        def _():
-            remote(
-                r_send.at[0, 0],
-                r_recv.at[e],
-                r_ssem.at[0],
-                r_rsem.at[e],
-                {"fs": e, "tp": y * SIDE + f % SIDE},
-            ).wait_recv()
+    def returned(count):
+        ref = r_recv.at[pl.ds(0, count)]
+        return remote(ref, ref, r_ssem.at[0], r_rsem.at[0], {"fs": (f + 1) % n_fs})
+
+    mine = f % SIDE == x
+
+    @pl.when(mine)
+    def _():
+        returned(n_fs - 1).wait_recv()
+
+    @pl.when(jnp.logical_not(mine))
+    def _():
+        returned(n_fs).wait_recv()
 
     back = r_recv[...].reshape(rows, fcols)
     mix = jnp.dot(high_v[...], back, preferred_element_type=F32) + jnp.dot(
         low_v[...], back, preferred_element_type=F32
     )
     mix_out[...] = mix.astype(BF)
-    for r in range(CHUNKS):
-        each_return(r, lambda c: c.wait_send())
+
+    @pl.when(mine)
+    def _():
+        returned(n_fs - 1).wait_send()
+
+    @pl.when(jnp.logical_not(mine))
+    def _():
+        returned(n_fs).wait_send()
 
 
 def copy_out(a, b, c, a_out, b_out, c_out, sems):
@@ -572,8 +568,9 @@
             pltpu.VMEM((tiles, 8, fcols), BF),
             pltpu.VMEM((n_tp, tiles, 8, fcols), BF),
             pltpu.VMEM((sources, SIDE, cap // 8, 8, hid), BF),
-            pltpu.VMEM((SIDE, SIDE, sources, cap // 8, 8, hid), BF),
+            pltpu.VMEM((n_tp, sources, cap // 8, 8, hid), BF),
             pltpu.VMEM((SIDE, SIDE, width // SIDE, hid), BF),
+            pltpu.VMEM((SIDE, SIDE * hid, width // SIDE), BF),
             pltpu.VMEM((SIDE, sources, cap // 8, 8, fcols), BF),
             pltpu.VMEM((ecount, cap // 8, 8, fcols), BF),
             pltpu.VMEM((ecount, tok), F32),
@@ -584,20 +581,20 @@
             pltpu.VMEM((tok, rows), BF),
             pltpu.VMEM((rows, 2 * hid), F32),
             dma((9,)),
-            dma((n_fs,)),
-            dma((n_fs,)),
-            dma((n_fs,)),
-            dma((n_fs,)),
-            dma((n_fs,)),
-            dma((n_fs,)),
+            dma((1,)),
+            dma((1,)),
+            dma((1,)),
+            dma((ecount // 4 + 1,)),
+            dma((1,)),
+            dma((1,)),
+            dma((1,)),
             dma((SIDE,)),
-            dma((SIDE,)),
-            dma((16,)),
-            dma((16,)),
-            dma((40,)),
-            dma((40,)),
-            dma((CHUNKS * n_tp,)),
-            dma((CHUNKS * n_tp,)),
+            dma((1,)),
+            dma((9,)),
+            dma((1,)),
+            dma((25,)),
+            dma((1,)),
+            dma((CHUNKS,)),
         ],
         compiler_params=pltpu.CompilerParams(
             collective_id=0, has_side_effects=True, vmem_limit_bytes=48 * 1024 * 1024

time: 98.2 us -> 89.9 us (0.915)
  Pallas kernels: 97 us -> 89.1 us
    pallas_call x1, Pallas kernels: 96 us -> 88.1 us  [on_device(): pl.pallas_call(functools.partial(kernel, n_fs, n_tp), out_shape=(jax.Shap...]
where the time goes in v6:
time: 89.9 us; the launch traced here: 89.8 us
  Pallas kernels  89.1 us (99%)
    pallas_call x1, Pallas kernels, on_device(): pl.pallas_call(functools.partial(kernel, n_fs, n_tp), out_shape=(jax.Shap...  88.1 us

profile of v6, /device:TPU:1, one launch (start us, length us, event | category | flops | bytes accessed | tf_op | source)
XLA Modules:
  0.0 89.8 jit_solution(8714257297143273348)
XLA Ops:
  0.6 88.1 %shard_map.94 = (bf16[32,64,128]{2,1,0:T(8,128)(2,1)S(1)}, bf16[32,64,128]{2,1,0:T(8,128)(2,1)S(1)}, bf16[128,128]{1,0:T(8,128)(2,1)S(1)}) custom-call(s32[4,128]{1,0:T(4,128)} %bitcast.10, f32[4,128]{1,0:T(4,128)} %bitcast.11, f32[16,128]{1,0:T(8,128)} %bitcast.9, bf16[128,2048]{1,0:T(8,128)(2,1)} %tokens_hbm.1, f32[32,64,128]{2,1,0:T(8,128)} %gate_hbm.1, ...), custom_call_target="tpu_custom_call" | custom-call | tf_op jit(solution)/shard_map/pallas_call | solution.py:549
  88.8 1.0 %shard_map.95 = (bf16[1,2048,128]{2,1,0:T(8,128)(2,1)}, bf16[1,2048,128]{2,1,0:T(8,128)(2,1)}, bf16[128,128]{1,0:T(8,128)(2,1)}) custom-call(bf16[1,2048,128]{2,1,0:T(8,128)(2,1)S(1)} %bitcast.6, bf16[1,2048,128]{2,1,0:T(8,128)(2,1)S(1)} %bitcast.7, bf16[128,128]{1,0:T(8,128)(2,1)S(1)} %get-tuple-element.8.c), custom_call_target="tpu_custom_call" | custom-call | tf_op jit(solution)/shard_map/pallas_call | solution.py:618

commit v7 on v6

--- a/solution.py
+++ b/solution.py
@@ -12,7 +12,7 @@
 BF = jnp.bfloat16
 F32 = jnp.float32
 MESH = pl.DeviceIdType.MESH
-CHUNKS = 4
+CHUNKS = 8
 SIDE = 4
 
 
@@ -154,6 +154,7 @@
     w_recv,
     t_send,
     t_grid,
+    t_rows,
     a_send,
     a_grid,
     d_grid,
@@ -355,6 +356,10 @@
     tg.rest()
     dx.whole(d_grid.at[0]).wait_recv()
 
+    @pl.loop(0, n_tp)
+    def _(b):
+        t_rows[b] = t_grid[b].reshape(rows, fcols)
+
     @pl.loop(0, SIDE)
     def _(p):
         for g in range(SIDE):
@@ -362,7 +367,7 @@
 
 
     def lhs(chip):
-        return t_grid[chip].reshape(rows, fcols)
+        return t_rows[chip]
 
     def rhs(chip):
         return w_recv[pl.ds(chip * 2, 2)].reshape(fcols, 2 * hid)
@@ -567,6 +572,7 @@
             pltpu.VMEM((ecount, stripe, 2 * hid), BF),
             pltpu.VMEM((tiles, 8, fcols), BF),
             pltpu.VMEM((n_tp, tiles, 8, fcols), BF),
+            pltpu.VMEM((n_tp, rows, fcols), BF),
             pltpu.VMEM((sources, SIDE, cap // 8, 8, hid), BF),
             pltpu.VMEM((n_tp, sources, cap // 8, 8, hid), BF),
             pltpu.VMEM((SIDE, SIDE, width // SIDE, hid), BF),

time: 89.9 us -> 90.3 us (level)
  no operation moved by 1% of the time
where the time goes in v7:
time: 90.3 us; the launch traced here: 90.2 us
  Pallas kernels  89.5 us (99%)
    pallas_call x1, Pallas kernels, on_device(): pl.pallas_call(functools.partial(kernel, n_fs, n_tp), out_shape=(jax.Shap...  88.5 us

profile of v7, /device:TPU:1, one launch (start us, length us, event | category | flops | bytes accessed | tf_op | source)
XLA Modules:
  0.0 90.2 jit_solution(16782060001907358548)
XLA Ops:
  0.6 88.5 %shard_map.94 = (bf16[32,64,128]{2,1,0:T(8,128)(2,1)S(1)}, bf16[32,64,128]{2,1,0:T(8,128)(2,1)S(1)}, bf16[128,128]{1,0:T(8,128)(2,1)S(1)}) custom-call(s32[4,128]{1,0:T(4,128)} %bitcast.10, f32[4,128]{1,0:T(4,128)} %bitcast.11, f32[16,128]{1,0:T(8,128)} %bitcast.9, bf16[128,2048]{1,0:T(8,128)(2,1)} %tokens_hbm.1, f32[32,64,128]{2,1,0:T(8,128)} %gate_hbm.1, ...), custom_call_target="tpu_custom_call" | custom-call | tf_op jit(solution)/shard_map/pallas_call | solution.py:554
  89.2 1.0 %shard_map.95 = (bf16[1,2048,128]{2,1,0:T(8,128)(2,1)}, bf16[1,2048,128]{2,1,0:T(8,128)(2,1)}, bf16[128,128]{1,0:T(8,128)(2,1)}) custom-call(bf16[1,2048,128]{2,1,0:T(8,128)(2,1)S(1)} %bitcast.6, bf16[1,2048,128]{2,1,0:T(8,128)(2,1)S(1)} %bitcast.7, bf16[128,128]{1,0:T(8,128)(2,1)S(1)} %get-tuple-element.8.c), custom_call_target="tpu_custom_call" | custom-call | tf_op jit(solution)/shard_map/pallas_call | solution.py:624

commit v8 on v7

--- a/solution.py
+++ b/solution.py
@@ -388,13 +388,6 @@
         weights_copy(2 * k, 0, 0, 4).wait_recv()
         multiply((z + n_z // 2 + k) % n_z, (z + n_z // 2 - k) % n_z)
 
-    stores = [
-        pltpu.make_async_copy(w_recv.at[:, :, pl.ds(0, hid)], gate_out, local_sems.at[7]),
-        pltpu.make_async_copy(w_recv.at[:, :, pl.ds(hid, hid)], linear_out, local_sems.at[8]),
-    ]
-    for store in stores:
-        store.start()
-
     n_q = a_send.shape[0]
     offsets = (4, 5, 3, 6, 2, 1, 7, 0)
     chunk = n_q // CHUNKS
@@ -434,6 +427,13 @@
         for dy_, dx_ in others:
             active_copy(r, ahead(dy_, dx_)).start()
     a_grid[t] = a_send[:, x]
+    stores = [
+        pltpu.make_async_copy(w_recv.at[:, :, pl.ds(0, hid)], gate_out, local_sems.at[7]),
+        pltpu.make_async_copy(w_recv.at[:, :, pl.ds(hid, hid)], linear_out, local_sems.at[8]),
+    ]
+    for store in stores:
+        store.start()
+
     share = chunk * span // SIDE
 
     def multiply_down(r):

time: 90.3 us -> 90.1 us (level)
  no operation moved by 1% of the time
where the time goes in v8:
time: 90.1 us; the launch traced here: 90 us
  Pallas kernels  89.3 us (99%)
    pallas_call x1, Pallas kernels, on_device(): pl.pallas_call(functools.partial(kernel, n_fs, n_tp), out_shape=(jax.Shap...  88.4 us

profile of v8, /device:TPU:1, one launch (start us, length us, event | category | flops | bytes accessed | tf_op | source)
XLA Modules:
  0.0 90.0 jit_solution(13134408437501473786)
XLA Ops:
  0.6 88.4 %shard_map.94 = (bf16[32,64,128]{2,1,0:T(8,128)(2,1)S(1)}, bf16[32,64,128]{2,1,0:T(8,128)(2,1)S(1)}, bf16[128,128]{1,0:T(8,128)(2,1)S(1)}) custom-call(s32[4,128]{1,0:T(4,128)} %bitcast.10, f32[4,128]{1,0:T(4,128)} %bitcast.11, f32[16,128]{1,0:T(8,128)} %bitcast.9, bf16[128,2048]{1,0:T(8,128)(2,1)} %tokens_hbm.1, f32[32,64,128]{2,1,0:T(8,128)} %gate_hbm.1, ...), custom_call_target="tpu_custom_call" | custom-call | tf_op jit(solution)/shard_map/pallas_call | solution.py:554
  89.0 1.0 %shard_map.95 = (bf16[1,2048,128]{2,1,0:T(8,128)(2,1)}, bf16[1,2048,128]{2,1,0:T(8,128)(2,1)}, bf16[128,128]{1,0:T(8,128)(2,1)}) custom-call(bf16[1,2048,128]{2,1,0:T(8,128)(2,1)S(1)} %bitcast.6, bf16[1,2048,128]{2,1,0:T(8,128)(2,1)S(1)} %bitcast.7, bf16[128,128]{1,0:T(8,128)(2,1)S(1)} %get-tuple-element.8.c), custom_call_target="tpu_custom_call" | custom-call | tf_op jit(solution)/shard_map/pallas_call | solution.py:624
